TPU v7x, 32 devices: a whole 2x2x4 slice. The times are simulated.
32 devices in a mesh: ep: 16 (over z, x, core), tp: 2 (over y).
Axes of the slice: x: 2, y: 2, z: 4, core: 2. Of those that a mesh axis runs over, the one named last changes fastest.
Arguments:
- tokens: bfloat16 [2048, 2048], P('ep'), may hold values from -6 to 6
- routes: int32 [2048, 2], P('ep'), may hold values from 0 to 3, all different within a row; in each aligned block of 128 rows (0 to 127, 128 to 255, ...) at most 80 rows name the same one
- router_weight: bfloat16 [2048, 4], replicated, may hold values from -0.125 to 0.125
- gate_proj: bfloat16 [16, 2048, 1024], P('ep', None, 'tp'), may hold values from -0.125 to 0.125
- up_proj: bfloat16 [16, 2048, 1024], P('ep', None, 'tp'), may hold values from -0.125 to 0.125
- down_proj: bfloat16 [16, 1024, 2048], P('ep', 'tp'), may hold values from -0.09375 to 0.09375
- cotangent: bfloat16 [2048, 2048], P('ep'), may hold values from -1.5 to 1.5
Outputs:
- token_grad: bfloat16 [2048, 2048], P('ep', 'tp')
- gate_grad: float32 [2048, 2], P('ep')
- router_grad: float32 [2048, 4], P('ep')
- gate_proj_grad: float32 [16, 2048, 1024], P('ep', None, 'tp')
- up_proj_grad: float32 [16, 2048, 1024], P('ep', None, 'tp')
- down_proj_grad: float32 [16, 1024, 2048], P('ep', 'tp')
Inputs may be any that keep to these rules, and one draw needn't show every extreme that they name: `routes`: each row names 2 different experts. Among the rows of one index of ep no expert is named more than 80 times, a bound that some block reaches.
All inputs are finite; a program needn't handle non-finite values.
Results may differ from a plain program's by a relative error of at most 0.0085.
Values may be sent and summed in bfloat16 or wider, within the bound.
A program may use at most 128 MiB of HBM per device.

v0:
```python
import functools

import jax
import jax.numpy as jnp
from jax import lax
from jax.experimental import pallas as pl
from jax.experimental.pallas import tpu as pltpu
from jax.sharding import Mesh, PartitionSpec as P

MEMBERS = 4
TOP = 2
LANES = 128
F32 = jnp.float32
BF16 = jnp.bfloat16
MESH = pl.DeviceIdType.MESH
NT = (((1,), (1,)), ((), ()))


def rows_kernel(
    share, send_ref, wg_hbm, wu_hbm, wd_hbm, x_hbm, dg_ref, du_ref, sc_ref, back_ref,
    full, wg_ref, wu_ref, wd_ref, out_sem, send_sem, recv_sem, load_sem,
):
    experts, n_m, n_tp, capacity, _ = full.shape
    e, m, t = lax.axis_index("e"), lax.axis_index("m"), lax.axis_index("tp")
    x_peer = lax.rem(m + 2, 4)
    core_peer = m + 1 - 2 * lax.rem(m, 2)
    held = n_m * capacity
    first_cols, last_cols = pl.ds(0, share), pl.ds(share, share + LANES)

    def ahead(j):
        return lax.rem(t + j, n_tp)

    def behind(j):
        return lax.rem(t + n_tp - j, n_tp)

    barrier = pltpu.get_barrier_semaphore()
    peers = [(lax.rem(e + k, experts), m, t) for k in range(1, experts)]
    peers += [(e, x_peer, t), (e, core_peer, t)] + [(e, m, ahead(j)) for j in range(1, n_tp)]
    for peer in peers:
        pl.semaphore_signal(barrier, inc=1, device_id=peer, device_id_type=MESH)
    loads = [
        pltpu.make_async_copy(src, dst, load_sem.at[n])
        for n, (src, dst) in enumerate(
            [(send_ref.at[e], full.at[0, m, t]), (wg_hbm, wg_ref), (wu_hbm, wu_ref), (wd_hbm, wd_ref)]
        )
    ]
    for load in loads:
        load.start()
    pl.semaphore_wait(barrier, len(peers))

    def remote(src, dst, kind, k, device):
        return pltpu.make_async_remote_copy(
            src_ref=src,
            dst_ref=dst,
            send_sem=send_sem.at[kind, k],
            recv_sem=recv_sem.at[kind, k],
            device_id=device,
            device_id_type=MESH,
        )

    def piece(k, src_m, src_t, cols=None):
        ref = full.at[k, src_m, src_t]
        return ref if cols is None else ref.at[:, cols]

    X, CORE_OWN, CORE_X = 0, 1, 2
    def y_kind(j): return 3 + (j - 1)
    def a_kind(j): return 3 + (n_tp - 1) + (j - 1)
    def b_kind(j): return 3 + 2 * (n_tp - 1) + (j - 1)
    def core_y(j): return 3 + 3 * (n_tp - 1) + (j - 1)
    def core_a(j): return 3 + 4 * (n_tp - 1) + (j - 1)
    def core_b(j): return 3 + 5 * (n_tp - 1) + (j - 1)
    Z = 3 + 6 * (n_tp - 1)

    def pass_on(ref, kind, k, device):
        remote(ref, ref, kind, k, device).start()

    def landed(ref, kind, k):
        remote(ref, ref, kind, k, (e, core_peer, t)).wait_recv()

    def sent(ref, kind, k):
        remote(ref, ref, kind, k, (e, core_peer, t)).wait_send()

    for k in range(1, experts):
        there = lax.rem(e + k, experts)
        remote(send_ref.at[there], full.at[k, m, t], Z, k, (there, m, t)).start()
    loads[0].wait()

    x_to, core_to = (e, x_peer, t), (e, core_peer, t)

    def own(k):
        mine = piece(k, m, t)
        @pl.when(k > 0)
        def _():
            landed(mine, Z, k)
        pass_on(mine, X, k, x_to)
        for j in range(1, n_tp):
            pass_on(mine, y_kind(j), k, (e, m, ahead(j)))
        pass_on(mine, CORE_OWN, k, core_to)

    def neighbours(k):
        across = piece(k, x_peer, t)
        landed(across, X, k)
        for j in range(1, n_tp):
            pass_on(piece(k, x_peer, t, last_cols), b_kind(j), k, (e, m, ahead(j)))
        pass_on(across, CORE_X, k, core_to)
        for j in range(1, n_tp):
            beside = piece(k, m, behind(j))
            landed(beside, y_kind(j), k)
            pass_on(piece(k, m, behind(j), first_cols), a_kind(j), k, x_to)
            pass_on(beside, core_y(j), k, core_to)

    def corners(k):
        for j in range(1, n_tp):
            for cols, kind, core in ((first_cols, a_kind, core_a), (last_cols, b_kind, core_b)):
                ref = piece(k, x_peer, behind(j), cols)
                landed(ref, kind(j), k)
                pass_on(ref, core(j), k, core_to)

    other_x = lax.rem(core_peer + 2, 4)

    def partner(k):
        landed(piece(k, core_peer, t), CORE_OWN, k)
        landed(piece(k, other_x, t), CORE_X, k)
        for j in range(1, n_tp):
            landed(piece(k, core_peer, behind(j)), core_y(j), k)
            landed(piece(k, other_x, behind(j), first_cols), core_a(j), k)
            landed(piece(k, other_x, behind(j), last_cols), core_b(j), k)
        pltpu.make_async_copy(full.at[k], x_hbm.at[k], out_sem.at[k]).start()

    def compute(k):
        def part(tp_at, base, size):
            return full[k, :, tp_at, :, base : base + size].reshape(held, size)

        def contract(base, w_ref, nt):
            total = None
            for tp_at in range(n_tp):
                cols = slice(tp_at * share, (tp_at + 1) * share)
                rows = part(tp_at, base, share)
                if nt:
                    term = lax.dot_general(rows, w_ref[0, :, cols], NT, preferred_element_type=F32)
                else:
                    term = jnp.dot(rows, w_ref[0, cols, :], preferred_element_type=F32)
                total = term if total is None else total + term
            return total

        gpre = contract(0, wg_ref, False)
        upre = contract(0, wu_ref, False)
        qvals = contract(share, wd_ref, True)
        extra = part(0, 2 * share, LANES).astype(F32)
        lane = lax.broadcasted_iota(jnp.int32, extra.shape, 1)
        weight = jnp.sum(jnp.where(lane == e, extra, 0.0), axis=1, keepdims=True)
        sig = jax.nn.sigmoid(gpre)
        silu_val = gpre * sig
        hidden = (silu_val * upre).astype(BF16).astype(F32)
        gate_part = jnp.sum(hidden * qvals, axis=1, keepdims=True)
        dhid = weight * qvals
        d_gate = (dhid * upre * sig * (1.0 + gpre * (1.0 - sig))).astype(BF16)
        d_up = (dhid * silu_val).astype(BF16)
        dg_ref[k] = d_gate
        du_ref[k] = d_up
        sc_ref[k] = (weight * hidden).astype(BF16)
        gate_lanes = jnp.where(lane == 0, gate_part, 0.0).astype(BF16)
        source = lax.rem(e + experts - k, experts)
        for tp_at in range(n_tp):
            cols = slice(tp_at * share, (tp_at + 1) * share)
            grad = lax.dot_general(d_gate, wg_ref[0, cols, :], NT, preferred_element_type=F32)
            grad = grad + lax.dot_general(d_up, wu_ref[0, cols, :], NT, preferred_element_type=F32)
            back_ref[:, tp_at, source, :, :share] = grad.astype(BF16).reshape(n_m, capacity, share)
            back_ref[:, tp_at, source, :, share:] = gate_lanes.reshape(n_m, capacity, LANES)

    def step(i, carry):
        pl.when(i < experts)(lambda: own(i))
        pl.when((i >= 1) & (i < experts + 1))(lambda: neighbours(i - 1))
        pl.when((i >= 2) & (i < experts + 2))(lambda: corners(i - 2))

        @pl.when(i == 3)
        def _():
            for load in loads[1:]:
                load.wait()

        @pl.when(i >= 3)
        def _():
            partner(i - 3)
            compute(i - 3)

        return carry

    lax.fori_loop(0, experts + 3, step, 0)

    def finish(k, carry):
        mine = piece(k, m, t)
        @pl.when(k > 0)
        def _():
            sent(mine, Z, k)
        sent(mine, X, k)
        sent(mine, CORE_OWN, k)
        sent(piece(k, x_peer, t), CORE_X, k)
        for j in range(1, n_tp):
            sent(mine, y_kind(j), k)
            sent(piece(k, x_peer, t, last_cols), b_kind(j), k)
            sent(piece(k, m, behind(j), first_cols), a_kind(j), k)
            sent(piece(k, m, behind(j)), core_y(j), k)
            sent(piece(k, x_peer, behind(j), first_cols), core_a(j), k)
            sent(piece(k, x_peer, behind(j), last_cols), core_b(j), k)
        pltpu.make_async_copy(full.at[k], x_hbm.at[k], out_sem.at[k]).wait()
        return carry

    lax.fori_loop(0, experts, finish, 0)


def grads_kernel(x_ref, c_ref, dg_ref, du_ref, sc_ref, gg_ref, gu_ref, gd_ref, sct):
    @pl.when(pl.program_id(0) == 0)
    def _():
        sct[...] = sc_ref[...].T

    tile = x_ref.shape[-1]
    rows = dg_ref.shape[0]
    xt = x_ref[:, :, 0].reshape(rows, tile).T
    gg_ref[0] = jnp.dot(xt, dg_ref[...], preferred_element_type=F32)
    gu_ref[0] = jnp.dot(xt, du_ref[...], preferred_element_type=F32)
    gd_ref[0] = jnp.dot(sct[...], c_ref[:, :, 0].reshape(rows, tile), preferred_element_type=F32)


def shards(tokens, routes, router_weight, gate_proj, up_proj, down_proj, cotangent):
    ntok, width = tokens.shape
    experts = router_weight.shape[1]
    n_m, n_tp = lax.axis_size("m"), lax.axis_size("tp")
    share = width // n_tp
    capacity = min(ntok, 5 * TOP * ntok // (4 * experts))
    capacity = -(-capacity // 16) * 16
    tp_index = lax.axis_index("tp")
    ff = gate_proj.shape[2]

    logits = jnp.dot(tokens, router_weight, preferred_element_type=F32)
    onehot = (routes[:, :, None] == jnp.arange(experts, dtype=jnp.int32)[None, None, :]).astype(F32)
    chosen = jnp.sum(onehot * logits[:, None, :], axis=2)
    first = jax.nn.sigmoid(chosen[:, 0] - chosen[:, 1])
    gates = jnp.stack([first, 1.0 - first], axis=1)
    used = gates.astype(BF16)
    named = jnp.sum(onehot, axis=1)
    below = (jnp.arange(ntok)[:, None] > jnp.arange(ntok)[None, :]).astype(BF16)
    rank = jnp.dot(below, named.astype(BF16), preferred_element_type=F32)
    slot = jnp.where(named > 0, rank, -1.0).astype(jnp.int32)
    place = (
        jnp.arange(capacity, dtype=jnp.int32)[None, :, None] == slot.T[:, None, :]
    ).astype(BF16)
    gate_cols = jnp.sum(onehot * used.astype(F32)[:, :, None], axis=1).astype(BF16)
    payload = jnp.concatenate(
        [
            lax.dynamic_slice_in_dim(tokens, tp_index * share, share, 1),
            lax.dynamic_slice_in_dim(cotangent, tp_index * share, share, 1),
            gate_cols,
            jnp.zeros((ntok, LANES - experts), BF16),
        ],
        axis=1,
    )
    rows = jnp.dot(
        place.reshape(experts * capacity, ntok), payload, preferred_element_type=F32
    ).astype(BF16)
    wide = 2 * share + LANES
    rows = rows.reshape(experts, capacity, wide)

    held = n_m * capacity
    back_wide = share + LANES
    hid_shape = jax.ShapeDtypeStruct((experts, held, ff), BF16)
    flops = 2 * experts * held * width * ff
    kinds = 4 + 6 * (n_tp - 1)
    vmem = pl.BlockSpec(memory_space=pltpu.VMEM)
    anywhere = pl.BlockSpec(memory_space=pl.ANY)
    full_shape = (experts, n_m, n_tp, capacity, wide)
    full, d_gate, d_up, scaled, back = pl.pallas_call(
        functools.partial(rows_kernel, share),
        in_specs=[vmem, anywhere, anywhere, anywhere],
        out_specs=[anywhere, vmem, vmem, vmem, vmem],
        out_shape=[
            jax.ShapeDtypeStruct(full_shape, BF16),
            hid_shape,
            hid_shape,
            hid_shape,
            jax.ShapeDtypeStruct((n_m, n_tp, experts, capacity, back_wide), BF16),
        ],
        scratch_shapes=[
            pltpu.VMEM(full_shape, BF16),
            pltpu.VMEM(gate_proj.shape, BF16),
            pltpu.VMEM(up_proj.shape, BF16),
            pltpu.VMEM(down_proj.shape, BF16),
            pltpu.SemaphoreType.DMA((experts,)),
            pltpu.SemaphoreType.DMA((kinds, experts)),
            pltpu.SemaphoreType.DMA((kinds, experts)),
            pltpu.SemaphoreType.DMA((4,)),
        ],
        compiler_params=pltpu.CompilerParams(
            collective_id=0, has_side_effects=True, vmem_limit_bytes=60 << 20
        ),
        cost_estimate=pl.CostEstimate(flops=5 * flops, bytes_accessed=30 << 20, transcendentals=0),
        name="rows",
    )(rows, gate_proj, up_proj, down_proj)

    mine = lax.psum_scatter(
        back.reshape(n_m * n_tp, experts * capacity, back_wide),
        ("m", "tp"),
        scatter_dimension=0,
        tiled=False,
    )

    tile = 256
    per = share // tile
    total = experts * held
    whole = lambda i: (0, 0)
    grad_gate, grad_up, grad_down = pl.pallas_call(
        grads_kernel,
        grid=(width // tile,),
        in_specs=[
            pl.BlockSpec((experts, n_m, 1, capacity, tile), lambda i: (0, 0, i // per, 0, i % per)),
            pl.BlockSpec((experts, n_m, 1, capacity, tile), lambda i: (0, 0, i // per, 0, per + i % per)),
            pl.BlockSpec((total, ff), whole),
            pl.BlockSpec((total, ff), whole),
            pl.BlockSpec((total, ff), whole),
        ],
        out_specs=[
            pl.BlockSpec((1, tile, ff), lambda i: (0, i, 0)),
            pl.BlockSpec((1, tile, ff), lambda i: (0, i, 0)),
            pl.BlockSpec((1, ff, tile), lambda i: (0, 0, i)),
        ],
        out_shape=[
            jax.ShapeDtypeStruct(gate_proj.shape, F32),
            jax.ShapeDtypeStruct(up_proj.shape, F32),
            jax.ShapeDtypeStruct(down_proj.shape, F32),
        ],
        scratch_shapes=[pltpu.VMEM((ff, total), BF16)],
        cost_estimate=pl.CostEstimate(flops=3 * flops, bytes_accessed=30 << 20, transcendentals=0),
        name="grads",
    )(full, full, d_gate.reshape(total, ff), d_up.reshape(total, ff), scaled.reshape(total, ff))

    home = lax.all_to_all(
        mine.reshape(experts, capacity, back_wide), "e", split_axis=0, concat_axis=0, tiled=True
    )
    route_sum = lax.dot_general(
        place.reshape(experts * capacity, ntok),
        home[:, :, :share].reshape(experts * capacity, share),
        (((0,), (0,)), ((), ())),
        preferred_element_type=F32,
    )
    gate_at = jnp.einsum(
        "ect,ecl->etl", place, home[:, :, share:], preferred_element_type=F32
    )[:, :, 0]
    gate_grad = jnp.sum(onehot * gate_at.T[:, None, :], axis=2)
    delta = first * (1.0 - first) * (gate_grad[:, 0] - gate_grad[:, 1])
    dlogits = delta[:, None] * (onehot[:, 0] - onehot[:, 1])
    router_rows = lax.dynamic_slice_in_dim(router_weight, tp_index * share, share, 0).astype(F32)
    router_part = lax.dot_general(dlogits, router_rows, NT, precision=lax.Precision.HIGHEST)
    token_grad = (route_sum + router_part).astype(BF16)
    n_ep = lax.axis_size("e") * n_m
    terms = lax.dot_general(
        dlogits, tokens.astype(F32), (((0,), (0,)), ((), ())), precision=lax.Precision.HIGHEST
    )
    terms = terms.reshape(experts, n_ep, width // n_ep).transpose(1, 0, 2)
    terms = lax.all_to_all(terms, ("e", "m"), split_axis=0, concat_axis=0, tiled=True)
    router_grad = jnp.sum(terms, axis=0).T
    return (token_grad, gate_grad, router_grad, grad_gate, grad_up, grad_down)


def solution(mesh):
    devices = mesh.devices
    grid = Mesh(
        devices.reshape(devices.shape[0] // MEMBERS, MEMBERS, devices.shape[1]), ("e", "m", "tp")
    )
    ep = ("e", "m")
    return jax.shard_map(
        shards,
        mesh=grid,
        in_specs=(
            P(ep, None),
            P(ep, None),
            P(),
            P(ep, None, "tp"),
            P(ep, None, "tp"),
            P(ep, "tp", None),
            P(ep, None),
        ),
        out_specs=(
            P(ep, "tp"),
            P(ep, None),
            P(ep, None),
            P(ep, None, "tp"),
            P(ep, None, "tp"),
            P(ep, "tp", None),
        ),
        check_vma=False,
    )
```

profile of v0, /device:TPU:0, one launch (start us, length us, event | category | flops | bytes accessed | tf_op | source)
XLA Modules:
  0.0 195.1 jit_solution(17979137370902010011)
XLA Ops:
  7.2 0.0 copy-start
  7.2 0.0 reduce-scatter.2.cloned.1.call-start
  7.2 0.7 copy-done
  7.9 1.3 fusion.19
  9.2 0.7 select_reduce_fusion.2
  9.9 0.1 eq.44
  10.0 0.7 select_reduce_fusion.1
  10.7 0.1 fusion.1
  10.8 0.1 copy.14
  11.0 0.1 bitcast_compare_fusion
  11.1 1.1 constant_dynamic-slice_fusion
  12.2 0.3 concatenate.8
  12.5 1.6 convolution_convert_fusion
  14.1 72.4 %rows.1 = (bf16[4,4,2,80,2176]{4,3,2,1,0:T(8,128)(2,1)}, bf16[4,320,512]{2,1,0:T(8,128)(2,1)}, bf16[4,320,512]{2,1,0:T(8,128)(2,1)}, bf16[4,320,512]{2,1,0:T(8,128)(2,1)}, bf16[4,2,4,80,1152]{4,3,2,1,0:T(8,128)(2,1)}) custom-call(bf16[4,80,2176]{2,1,0:T(8,128)(2,1)} %bitcast.37, bf16[1,2048,512]{2,1,0:T(8,128)(2,1)} %wg_hbm.1, bf16[1,2048,512]{2,1,0:T(8,128)(2,1)} %wu_hbm.1, ...), custom_call_target="tpu_custom_call" | custom-call | flops 13421772800 | bytes 31457280 | tf_op jit(solution)/shard_map/rows/pallas_call | solution.py:271
  86.5 0.0 copy-start.1
  86.5 0.0 reduce-scatter.2.cloned.1.call-update
  86.5 0.0 copy-start.2
  86.5 65.9 %reduce-scatter.2.cloned.1.call-done = bf16[1,320,1152]{2,1,0:T(8,128)(2,1)} async-done(((bf16[8,320,1152]{2,1,0:T(8,128)(2,1)}), bf16[1,320,1152]{2,1,0:T(8,128)(2,1)}) %reduce-scatter.2.cloned.1.call-update) | async-done | bytes 737296 | tf_op jit(solution)/shard_map/reduce_scatter | solution.py:299
  152.4 4.6 %all-to-all-start = ((bf16[4,80,1152]{2,1,0:T(8,128)(2,1)}), bf16[4,80,1152]{2,1,0:T(8,128)(2,1)S(1)}, u32[]{:S(2)}, u32[]{:S(2)}) async-start(bf16[4,80,1152]{2,1,0:T(8,128)(2,1)} %bitcast.38), calls=%async_computation.1 | async-start | bytes 1474560 | tf_op jit(solution)/shard_map/all_to_all | solution.py:335
  157.0 0.0 copy-done.1
  157.0 0.3 copy.16
  157.2 0.0 copy-done.2
  157.3 14.7 %grads.1 = (f32[1,2048,512]{2,1,0:T(8,128)}, f32[1,2048,512]{2,1,0:T(8,128)}, f32[1,512,2048]{2,1,0:T(8,128)}) custom-call(bf16[4,4,2,80,2176]{4,3,2,1,0:T(8,128)(2,1)} %get-tuple-element.15.x_ref.c_ref, bf16[4,4,2,80,2176]{4,3,2,1,0:T(8,128)(2,1)} %get-tuple-element.15.x_ref.c_ref, bf16[1280,512]{1,0:T(8,128)(2,1)} %bitcast.41, bf16[1280,512]{1,0:T(8,128)(2,1)} %bitcast.42, ...), custom_call_target="tpu_custom_call" | custom-call | flops 8053063680 | bytes 31457280 | tf_op jit(solution)/shard_map/grads/pallas_call | solution.py:310
  171.9 3.9 %all-to-all-done = bf16[4,80,1152]{2,1,0:T(8,128)(2,1)S(1)} async-done(((bf16[4,80,1152]{2,1,0:T(8,128)(2,1)}), bf16[4,80,1152]{2,1,0:T(8,128)(2,1)S(1)}, u32[]{:S(2)}, u32[]{:S(2)}) %all-to-all-start) | async-done | bytes 737312 | tf_op jit(solution)/shard_map/all_to_all | solution.py:335
  175.9 0.2 fusion.3
  176.1 0.0 copy-start.3
  176.1 1.1 convolution_bitcast_fusion.1
  177.2 3.8 %all-to-all-start.1 = ((f32[16,4,128]{2,1,0:T(4,128)}), f32[16,4,128]{2,1,0:T(4,128)S(1)}, u32[]{:S(2)}, u32[]{:S(2)}) async-start(f32[16,4,128]{2,1,0:T(4,128)} %convolution_bitcast_fusion.1), calls=%async_computation.2 | async-start | bytes 65536 | tf_op jit(solution)/shard_map/all_to_all | solution.py:358
  181.0 0.3 convolution_bitcast_fusion
  181.3 1.2 fusion
  182.5 5.1 %all-to-all-done.1 = f32[16,4,128]{2,1,0:T(4,128)S(1)} async-done(((f32[16,4,128]{2,1,0:T(4,128)}), f32[16,4,128]{2,1,0:T(4,128)S(1)}, u32[]{:S(2)}, u32[]{:S(2)}) %all-to-all-start.1) | async-done | bytes 32800 | tf_op jit(solution)/shard_map/all_to_all | solution.py:358
  187.6 0.6 reduce_sum.49
  188.2 0.0 copy-done.3
  (8 shorter events, 0.1 us)
Async XLA Ops:
  7.2 0.7 copy-start
  7.2 145.2 %reduce-scatter.2.cloned.1.call-start = ((), (), s32[]{:S(2)}) async-start(), calls=%async_computation.3 | async-start | bytes 6635520 | tf_op jit(solution)/shard_map/reduce_scatter | solution.py:299
  86.5 70.5 %copy-start.1 = (bf16[128,2048]{1,0:T(8,128)(2,1)S(1)}, bf16[128,2048]{1,0:T(8,128)(2,1)}, u32[]{:S(2)}) copy-start(bf16[128,2048]{1,0:T(8,128)(2,1)} %param.7) | copy-start | bytes 1572868
  86.5 70.8 %copy-start.2 = (s32[128,2]{0,1:T(2,128)S(1)}, s32[128,2]{0,1:T(2,128)}, u32[]{:S(2)}) copy-start(s32[128,2]{0,1:T(2,128)} %param.8) | copy-start | bytes 3076
  152.4 23.5 %all-to-all-start = ((bf16[4,80,1152]{2,1,0:T(8,128)(2,1)}), bf16[4,80,1152]{2,1,0:T(8,128)(2,1)S(1)}, u32[]{:S(2)}, u32[]{:S(2)}) async-start(bf16[4,80,1152]{2,1,0:T(8,128)(2,1)} %bitcast.38), calls=%async_computation.1 | async-start | bytes 1474560 | tf_op jit(solution)/shard_map/all_to_all | solution.py:335
  176.1 12.2 %copy-start.3 = (f32[128,2]{0,1:T(2,128)}, f32[128,2]{0,1:T(2,128)S(1)}, u32[]{:S(2)}) copy-start(f32[128,2]{0,1:T(2,128)S(1)} %select_reduce_fusion) | copy-start | bytes 3076
  177.2 10.4 %all-to-all-start.1 = ((f32[16,4,128]{2,1,0:T(4,128)}), f32[16,4,128]{2,1,0:T(4,128)S(1)}, u32[]{:S(2)}, u32[]{:S(2)}) async-start(f32[16,4,128]{2,1,0:T(4,128)} %convolution_bitcast_fusion.1), calls=%async_computation.2 | async-start | bytes 65536 | tf_op jit(solution)/shard_map/all_to_all | solution.py:358
Sparse Core Ops, SparseCore 0:
  86.6 65.7 reduce-scatter.1
where the time goes:
time: 196 us; the launch traced here: 195 us
  Pallas kernels  87 us (44%)
  waiting for transfers between devices  74.9 us (38%)
  between operations  14.2 us (7%)
  starting transfers between devices  8.4 us (4%)
  matrix products  5.82 us (3%)
  local copies, waits for them, and re-layouts  2.52 us (1%)
  other arithmetic  2.19 us (1%)
    pallas_call x1, Pallas kernels, shards(): pl.pallas_call(functools.partial(rows_kernel, share), in_specs=[vmem, any...  72.4 us
    reduce_scatter x1, waiting for transfers between devices, shards(): lax.psum_scatter(back.reshape(n_m * n_tp, experts * capacity, back_wide),...  65.9 us
    pallas_call x1, Pallas kernels, shards(): pl.pallas_call(grads_kernel, grid=(width // tile,), in_specs=[pl.BlockSpe...  14.7 us
    all_to_all x1, waiting for transfers between devices, shards(): lax.all_to_all(terms, ('e', 'm'), split_axis=0, concat_axis=0, tiled=True)  5.13 us
    all_to_all x1, starting transfers between devices, shards(): lax.all_to_all(mine.reshape(experts, capacity, back_wide), 'e', split_axi...  4.59 us
  transfers between devices with their start and end apart: 3, of which 3 were waited for; matrix products, arithmetic and copies ran while one was open for 1% of the time, Pallas kernels for 8%

commit v1 on v0

--- a/solution.py
+++ b/solution.py
@@ -17,15 +17,24 @@
 
 
 def rows_kernel(
-    share, send_ref, wg_hbm, wu_hbm, wd_hbm, x_hbm, dg_ref, du_ref, sc_ref, back_ref,
-    full, wg_ref, wu_ref, wd_ref, out_sem, send_sem, recv_sem, load_sem,
+    share, send_ref, tok_ref, slot_ref, oh_ref, first_ref, rw_ref, wg_hbm, wu_hbm, wd_hbm,
+    x_hbm, dg_hbm, du_hbm, sc_hbm, grad_ref, gate_ref, router_ref,
+    full, wg_ref, wu_ref, wd_ref, dg_ref, du_ref, sc_ref, back, core_in, xa_in, yb_in, ya_in, xb_in, home, place,
+    gacc, gcore, gcore_in, gx_in, gt, gz, terms, terms_in,
+    out_sem, hid_sem, send_sem, recv_sem, load_sem, gsend, grecv, tsend, trecv,
 ):
     experts, n_m, n_tp, capacity, _ = full.shape
+    ntok, width = tok_ref.shape
+    half = share // 2
     e, m, t = lax.axis_index("e"), lax.axis_index("m"), lax.axis_index("tp")
+    n_ep = experts * n_m
+    me = e * n_m + m
+    x_half, core = lax.div(m, 2), lax.rem(m, 2)
     x_peer = lax.rem(m + 2, 4)
-    core_peer = m + 1 - 2 * lax.rem(m, 2)
+    core_peer = m + 1 - 2 * core
     held = n_m * capacity
     first_cols, last_cols = pl.ds(0, share), pl.ds(share, share + LANES)
+    low, high = pl.ds(0, half), pl.ds(half, share - half)
 
     def ahead(j):
         return lax.rem(t + j, n_tp)
@@ -33,11 +42,15 @@
     def behind(j):
         return lax.rem(t + n_tp - j, n_tp)
 
+    def ep_at(d):
+        there = lax.rem(me + d, n_ep)
+        return (lax.div(there, n_m), lax.rem(there, n_m), t)
+
     barrier = pltpu.get_barrier_semaphore()
-    peers = [(lax.rem(e + k, experts), m, t) for k in range(1, experts)]
-    peers += [(e, x_peer, t), (e, core_peer, t)] + [(e, m, ahead(j)) for j in range(1, n_tp)]
-    for peer in peers:
-        pl.semaphore_signal(barrier, inc=1, device_id=peer, device_id_type=MESH)
+    for d in range(1, n_ep):
+        pl.semaphore_signal(barrier, inc=1, device_id=ep_at(d), device_id_type=MESH)
+    for j in range(1, n_tp):
+        pl.semaphore_signal(barrier, inc=1, device_id=(e, m, ahead(j)), device_id_type=MESH)
     loads = [
         pltpu.make_async_copy(src, dst, load_sem.at[n])
         for n, (src, dst) in enumerate(
@@ -46,7 +59,7 @@
     ]
     for load in loads:
         load.start()
-    pl.semaphore_wait(barrier, len(peers))
+    pl.semaphore_wait(barrier, n_ep - 1 + n_tp - 1)
 
     def remote(src, dst, kind, k, device):
         return pltpu.make_async_remote_copy(
@@ -62,40 +75,49 @@
         ref = full.at[k, src_m, src_t]
         return ref if cols is None else ref.at[:, cols]
 
-    X, CORE_OWN, CORE_X = 0, 1, 2
-    def y_kind(j): return 3 + (j - 1)
-    def a_kind(j): return 3 + (n_tp - 1) + (j - 1)
-    def b_kind(j): return 3 + 2 * (n_tp - 1) + (j - 1)
-    def core_y(j): return 3 + 3 * (n_tp - 1) + (j - 1)
-    def core_a(j): return 3 + 4 * (n_tp - 1) + (j - 1)
-    def core_b(j): return 3 + 5 * (n_tp - 1) + (j - 1)
-    Z = 3 + 6 * (n_tp - 1)
+    others = n_tp - 1
+    X, CORE_OWN, CORE_X, Z, R1, R2A, R3B, RET = range(8)
+    def y_kind(j): return 8 + (j - 1)
+    def a_kind(j): return 8 + others + (j - 1)
+    def b_kind(j): return 8 + 2 * others + (j - 1)
+    def core_y(j): return 8 + 3 * others + (j - 1)
+    def core_a(j): return 8 + 4 * others + (j - 1)
+    def core_b(j): return 8 + 5 * others + (j - 1)
+    def r2b(j): return 8 + 6 * others + (j - 1)
+    def r3a(j): return 8 + 7 * others + (j - 1)
+
+    x_to, core_to = (e, x_peer, t), (e, core_peer, t)
 
     def pass_on(ref, kind, k, device):
         remote(ref, ref, kind, k, device).start()
 
     def landed(ref, kind, k):
-        remote(ref, ref, kind, k, (e, core_peer, t)).wait_recv()
+        remote(ref, ref, kind, k, core_to).wait_recv()
 
     def sent(ref, kind, k):
-        remote(ref, ref, kind, k, (e, core_peer, t)).wait_send()
+        remote(ref, ref, kind, k, core_to).wait_send()
 
     for k in range(1, experts):
         there = lax.rem(e + k, experts)
         remote(send_ref.at[there], full.at[k, m, t], Z, k, (there, m, t)).start()
-    loads[0].wait()
-
-    x_to, core_to = (e, x_peer, t), (e, core_peer, t)
 
     def own(k):
         mine = piece(k, m, t)
         @pl.when(k > 0)
         def _():
             landed(mine, Z, k)
-        pass_on(mine, X, k, x_to)
-        for j in range(1, n_tp):
-            pass_on(mine, y_kind(j), k, (e, m, ahead(j)))
-        pass_on(mine, CORE_OWN, k, core_to)
+            pass_on(mine, X, k, x_to)
+            for j in range(1, n_tp):
+                pass_on(mine, y_kind(j), k, (e, m, ahead(j)))
+            pass_on(mine, CORE_OWN, k, core_to)
+
+        @pl.when(k == 0)
+        def _():
+            src = send_ref.at[e]
+            remote(src, mine, X, 0, x_to).start()
+            for j in range(1, n_tp):
+                remote(src, mine, y_kind(j), 0, (e, m, ahead(j))).start()
+            remote(src, mine, CORE_OWN, 0, core_to).start()
 
     def neighbours(k):
         across = piece(k, x_peer, t)
@@ -111,10 +133,10 @@
 
     def corners(k):
         for j in range(1, n_tp):
-            for cols, kind, core in ((first_cols, a_kind, core_a), (last_cols, b_kind, core_b)):
+            for cols, kind, across in ((first_cols, a_kind, core_a), (last_cols, b_kind, core_b)):
                 ref = piece(k, x_peer, behind(j), cols)
                 landed(ref, kind(j), k)
-                pass_on(ref, core(j), k, core_to)
+                pass_on(ref, across(j), k, core_to)
 
     other_x = lax.rem(core_peer + 2, 4)
 
@@ -126,6 +148,10 @@
             landed(piece(k, other_x, behind(j), first_cols), core_a(j), k)
             landed(piece(k, other_x, behind(j), last_cols), core_b(j), k)
         pltpu.make_async_copy(full.at[k], x_hbm.at[k], out_sem.at[k]).start()
+
+    def hidden_copies(k):
+        pairs = ((dg_ref, dg_hbm), (du_ref, du_hbm), (sc_ref, sc_hbm))
+        return [pltpu.make_async_copy(a.at[k], b.at[k], hid_sem.at[n, k]) for n, (a, b) in enumerate(pairs)]
 
     def compute(k):
         def part(tp_at, base, size):
@@ -159,42 +185,229 @@
         dg_ref[k] = d_gate
         du_ref[k] = d_up
         sc_ref[k] = (weight * hidden).astype(BF16)
-        gate_lanes = jnp.where(lane == 0, gate_part, 0.0).astype(BF16)
+        for copy in hidden_copies(k):
+            copy.start()
         source = lax.rem(e + experts - k, experts)
+        gate_lanes = jnp.where(lane == source, gate_part, 0.0).reshape(n_m, capacity, LANES)
+        for at in range(n_m):
+            gacc[at % 2, at // 2, :capacity, :] += gate_lanes[at]
         for tp_at in range(n_tp):
             cols = slice(tp_at * share, (tp_at + 1) * share)
             grad = lax.dot_general(d_gate, wg_ref[0, cols, :], NT, preferred_element_type=F32)
             grad = grad + lax.dot_general(d_up, wu_ref[0, cols, :], NT, preferred_element_type=F32)
-            back_ref[:, tp_at, source, :, :share] = grad.astype(BF16).reshape(n_m, capacity, share)
-            back_ref[:, tp_at, source, :, share:] = gate_lanes.reshape(n_m, capacity, LANES)
+            grad = grad.astype(BF16).reshape(n_m, capacity, share)
+            for at in range(n_m):
+                back[k, at % 2, at // 2, tp_at] = grad[at]
+        remote(back.at[k, 1 - core], core_in.at[k], R1, k, core_to).start()
+
+    def add(*terms):
+        total = terms[0].astype(F32)
+        for term in terms[1:]:
+            total = total + term.astype(F32)
+        return total.astype(BF16)
+
+    x_other = 1 - x_half
+
+    def across_a(k):
+        return back.at[k, core, x_other, :, :, low]
+
+    def across_b(k, j):
+        return back.at[k, core, :, ahead(j), :, high]
+
+    def reduce_first(k):
+        landed(core_in.at[k], R1, k)
+        back[k, core] = add(back[k, core], core_in[k])
+        remote(across_a(k), xa_in.at[k], R2A, k, x_to).start()
+        for j in range(1, n_tp):
+            remote(across_b(k, j), yb_in.at[k, j - 1], r2b(j), k, (e, m, ahead(j))).start()
+
+    def onward_a(k, j):
+        return back.at[k, core, x_half, ahead(j), :, low]
+
+    def onward_b(k):
+        return back.at[k, core, x_other, t, :, high]
+
+    def reduce_second(k):
+        landed(xa_in.at[k], R2A, k)
+        for j in range(1, n_tp):
+            onward_a(k, j)[...] = add(onward_a(k, j)[...], xa_in[k, ahead(j)])
+            remote(onward_a(k, j), ya_in.at[k, j - 1], r3a(j), k, (e, m, ahead(j))).start()
+        for j in range(1, n_tp):
+            landed(yb_in.at[k, j - 1], r2b(j), k)
+        onward_b(k)[...] = add(onward_b(k)[...], *[yb_in[k, j - 1, x_other] for j in range(1, n_tp)])
+        remote(onward_b(k), xb_in.at[k], R3B, k, x_to).start()
+
+    def mine_back(k):
+        return back.at[k, core, x_half, t]
+
+    def reduce_third(k):
+        for j in range(1, n_tp):
+            landed(ya_in.at[k, j - 1], r3a(j), k)
+        landed(xb_in.at[k], R3B, k)
+        ref = mine_back(k)
+        ref[:, :half] = add(ref[:, :half], xa_in[k, t], *[ya_in[k, j - 1] for j in range(1, n_tp)])
+        ref[:, half:] = add(ref[:, half:], xb_in[k], *[yb_in[k, j - 1, x_half] for j in range(1, n_tp)])
+
+        def away():
+            there = lax.rem(e + experts - k, experts)
+            remote(ref, home.at[e], RET, k, (there, m, t)).start()
+
+        def here():
+            home[e] = ref[...]
+
+        if isinstance(k, int):
+            (away if k else here)()
+        else:
+            pl.when(k > 0)(away)
+            pl.when(k == 0)(here)
+
+    gacc[...] = jnp.zeros_like(gacc)
 
     def step(i, carry):
         pl.when(i < experts)(lambda: own(i))
         pl.when((i >= 1) & (i < experts + 1))(lambda: neighbours(i - 1))
-        pl.when((i >= 2) & (i < experts + 2))(lambda: corners(i - 2))
-
-        @pl.when(i == 3)
+        pl.when(i >= 3)(lambda: reduce_first(i - 3))
+        pl.when(i >= 4)(lambda: reduce_second(i - 4))
+        pl.when(i >= 5)(lambda: reduce_third(i - 5))
+
+        @pl.when(i == 2)
         def _():
-            for load in loads[1:]:
+            for load in loads:
                 load.wait()
 
-        @pl.when(i >= 3)
+        @pl.when(i >= 2)
         def _():
-            partner(i - 3)
-            compute(i - 3)
+            corners(i - 2)
+            partner(i - 2)
+            compute(i - 2)
 
         return carry
 
-    lax.fori_loop(0, experts + 3, step, 0)
+    lax.fori_loop(0, experts + 2, step, 0)
+
+    def gate_copy(src, dst, n, device):
+        return pltpu.make_async_remote_copy(
+            src_ref=src,
+            dst_ref=dst,
+            send_sem=gsend.at[n],
+            recv_sem=grecv.at[n],
+            device_id=device,
+            device_id_type=MESH,
+        )
+
+    erows = gcore.shape[2]
+    last = experts - 1
+    for at in range(n_m):
+        gcore[at % 2, at // 2] = gacc[at % 2, at // 2].T[:erows]
+    to_core = gate_copy(gcore.at[1 - core], gcore_in, 0, core_to)
+    to_core.start()
+    reduce_first(last)
+    to_core.wait_recv()
+    gcore[core] = gcore[core] + gcore_in[...]
+    to_x = gate_copy(gcore.at[core, x_other], gx_in, 1, x_to)
+    to_x.start()
+    reduce_second(last - 1)
+    reduce_third(last - 2)
+    to_x.wait_recv()
+    gt[t] = gcore[core, x_half] + gx_in[...]
+    to_t = [gate_copy(gt.at[t], gt.at[t], 1 + j, (e, m, ahead(j))) for j in range(1, n_tp)]
+    for copy in to_t:
+        copy.start()
+    reduce_second(last)
+    reduce_third(last - 1)
+    for j in range(1, n_tp):
+        gate_copy(gt.at[behind(j)], gt.at[behind(j)], 1 + j, (e, m, ahead(j))).wait_recv()
+    whole = gt[0]
+    for j in range(1, n_tp):
+        whole = whole + gt[j]
+    gz[e] = whole
+    to_z = [
+        gate_copy(gz.at[e], gz.at[e], n_tp + k, (lax.rem(e + k, experts), m, t)) for k in range(1, experts)
+    ]
+    for copy in to_z:
+        copy.start()
+    for at in range(experts):
+        rows = lax.broadcasted_iota(jnp.int32, (capacity, ntok), 0)
+        place[at] = jnp.where(rows == slot_ref[at : at + 1, :], 1.0, 0.0).astype(BF16)
+    reduce_third(last)
+    for k in range(1, experts):
+        src = gz.at[lax.rem(e + experts - k, experts)]
+        gate_copy(src, src, n_tp + k, core_to).wait_recv()
+
+    HIGHEST = lax.Precision.HIGHEST
+    gates = []
+    row = lax.broadcasted_iota(jnp.int32, gz.shape[1:], 0)
+    for at in range(experts):
+        line = jnp.sum(jnp.where(row == e, gz[at], 0.0), axis=0, keepdims=True)
+        line = jnp.broadcast_to(line, (8, LANES))[:, :capacity]
+        got = jnp.dot(line, place[at].astype(F32), precision=HIGHEST, preferred_element_type=F32)
+        gates.append(got[0:1])
+    picks = [[oh_ref[n, at : at + 1, :] for at in range(experts)] for n in range(TOP)]
+    gate = [sum(picks[n][at] * gates[at] for at in range(experts)) for n in range(TOP)]
+    first = first_ref[...]
+    delta = first * (1.0 - first) * (gate[0] - gate[1])
+    gate_ref[0:1] = gate[0]
+    gate_ref[1:2] = gate[1]
+    pad = -experts % 8
+    zero = [jnp.zeros((pad, ntok), F32)] if pad else []
+    dlog = jnp.concatenate([delta * (picks[0][at] - picks[1][at]) for at in range(experts)] + zero, axis=0)
+    term = jnp.dot(dlog, tok_ref[...].astype(F32), precision=HIGHEST, preferred_element_type=F32)
+    cols = width // n_ep
+    for at in range(n_ep):
+        terms[at, :, :cols] = term[:, at * cols : (at + 1) * cols]
+
+    def term_copy(d):
+        there = lax.rem(me + d, n_ep)
+        return pltpu.make_async_remote_copy(
+            src_ref=terms.at[there],
+            dst_ref=terms_in.at[d],
+            send_sem=tsend.at[d],
+            recv_sem=trecv.at[d],
+            device_id=ep_at(d),
+            device_id_type=MESH,
+        )
+
+    def each(d, carry):
+        term_copy(d).start()
+        return carry
+
+    lax.fori_loop(1, n_ep, each, 0)
+
+    router_part = lax.dot_general(
+        dlog, rw_ref[...], (((0,), (0,)), ((), ())), precision=HIGHEST, preferred_element_type=F32
+    )
+    spread = place[...].reshape(experts * capacity, ntok).T
+    for k in range(1, experts):
+        landed(home.at[lax.rem(e + k, experts)], RET, k)
+    route_sum = jnp.dot(spread, home[...].reshape(experts * capacity, share), preferred_element_type=F32)
+    grad_ref[...] = (route_sum + router_part).astype(BF16)
+
+    def gather(d, total):
+        term_copy(d).wait_recv()
+        return total + terms_in[d, :, :cols]
+
+    router_ref[...] = lax.fori_loop(1, n_ep, gather, terms[me, :, :cols])
+
+    def done(d, carry):
+        term_copy(d).wait_send()
+        return carry
+
+    lax.fori_loop(1, n_ep, done, 0)
+    for copy in [to_core, to_x] + to_t + to_z:
+        copy.wait_send()
 
     def finish(k, carry):
         mine = piece(k, m, t)
         @pl.when(k > 0)
         def _():
             sent(mine, Z, k)
+            sent(mine_back(k), RET, k)
         sent(mine, X, k)
         sent(mine, CORE_OWN, k)
         sent(piece(k, x_peer, t), CORE_X, k)
+        sent(core_in.at[k], R1, k)
+        sent(across_a(k), R2A, k)
+        sent(onward_b(k), R3B, k)
         for j in range(1, n_tp):
             sent(mine, y_kind(j), k)
             sent(piece(k, x_peer, t, last_cols), b_kind(j), k)
@@ -202,7 +415,11 @@
             sent(piece(k, m, behind(j)), core_y(j), k)
             sent(piece(k, x_peer, behind(j), first_cols), core_a(j), k)
             sent(piece(k, x_peer, behind(j), last_cols), core_b(j), k)
+            sent(across_b(k, j), r2b(j), k)
+            sent(onward_a(k, j), r3a(j), k)
         pltpu.make_async_copy(full.at[k], x_hbm.at[k], out_sem.at[k]).wait()
+        for copy in hidden_copies(k):
+            copy.wait()
         return carry
 
     lax.fori_loop(0, experts, finish, 0)
@@ -261,46 +478,80 @@
     rows = rows.reshape(experts, capacity, wide)
 
     held = n_m * capacity
-    back_wide = share + LANES
     hid_shape = jax.ShapeDtypeStruct((experts, held, ff), BF16)
     flops = 2 * experts * held * width * ff
-    kinds = 4 + 6 * (n_tp - 1)
+    kinds = 8 + 8 * (n_tp - 1)
+    n_ep = experts * n_m
+    half = share // 2
+    erows = -(-experts // 8) * 8
+    cols = width // n_ep
+    router_rows = lax.dynamic_slice_in_dim(router_weight, tp_index * share, share, 0).astype(F32).T
+    router_rows = jnp.pad(router_rows, ((0, erows - experts), (0, 0)))
     vmem = pl.BlockSpec(memory_space=pltpu.VMEM)
     anywhere = pl.BlockSpec(memory_space=pl.ANY)
     full_shape = (experts, n_m, n_tp, capacity, wide)
-    full, d_gate, d_up, scaled, back = pl.pallas_call(
+    full, d_gate, d_up, scaled, token_grad, gate_rows, router_rows_out = pl.pallas_call(
         functools.partial(rows_kernel, share),
-        in_specs=[vmem, anywhere, anywhere, anywhere],
-        out_specs=[anywhere, vmem, vmem, vmem, vmem],
+        in_specs=[vmem] * 6 + [anywhere] * 3,
+        out_specs=[anywhere] * 4 + [vmem] * 3,
         out_shape=[
             jax.ShapeDtypeStruct(full_shape, BF16),
             hid_shape,
             hid_shape,
             hid_shape,
-            jax.ShapeDtypeStruct((n_m, n_tp, experts, capacity, back_wide), BF16),
+            jax.ShapeDtypeStruct((ntok, share), BF16),
+            jax.ShapeDtypeStruct((TOP, ntok), F32),
+            jax.ShapeDtypeStruct((erows, cols), F32),
         ],
         scratch_shapes=[
             pltpu.VMEM(full_shape, BF16),
             pltpu.VMEM(gate_proj.shape, BF16),
             pltpu.VMEM(up_proj.shape, BF16),
             pltpu.VMEM(down_proj.shape, BF16),
+            pltpu.VMEM(hid_shape.shape, BF16),
+            pltpu.VMEM(hid_shape.shape, BF16),
+            pltpu.VMEM(hid_shape.shape, BF16),
+            pltpu.VMEM((experts, 2, 2, n_tp, capacity, share), BF16),
+            pltpu.VMEM((experts, 2, n_tp, capacity, share), BF16),
+            pltpu.VMEM((experts, n_tp, capacity, half), BF16),
+            pltpu.VMEM((experts, n_tp - 1, 2, capacity, share - half), BF16),
+            pltpu.VMEM((experts, n_tp - 1, capacity, half), BF16),
+            pltpu.VMEM((experts, capacity, share - half), BF16),
+            pltpu.VMEM((experts, capacity, share), BF16),
+            pltpu.VMEM((experts, capacity, ntok), BF16),
+            pltpu.VMEM((2, 2, LANES, LANES), F32),
+            pltpu.VMEM((2, 2, erows, LANES), F32),
+            pltpu.VMEM((2, erows, LANES), F32),
+            pltpu.VMEM((erows, LANES), F32),
+            pltpu.VMEM((n_tp, erows, LANES), F32),
+            pltpu.VMEM((experts, erows, LANES), F32),
+            pltpu.VMEM((n_ep, erows, LANES), F32),
+            pltpu.VMEM((n_ep, erows, LANES), F32),
             pltpu.SemaphoreType.DMA((experts,)),
+            pltpu.SemaphoreType.DMA((3, experts)),
             pltpu.SemaphoreType.DMA((kinds, experts)),
             pltpu.SemaphoreType.DMA((kinds, experts)),
             pltpu.SemaphoreType.DMA((4,)),
+            pltpu.SemaphoreType.DMA((n_tp + experts,)),
+            pltpu.SemaphoreType.DMA((n_tp + experts,)),
+            pltpu.SemaphoreType.DMA((n_ep,)),
+            pltpu.SemaphoreType.DMA((n_ep,)),
         ],
         compiler_params=pltpu.CompilerParams(
             collective_id=0, has_side_effects=True, vmem_limit_bytes=60 << 20
         ),
         cost_estimate=pl.CostEstimate(flops=5 * flops, bytes_accessed=30 << 20, transcendentals=0),
         name="rows",
-    )(rows, gate_proj, up_proj, down_proj)
-
-    mine = lax.psum_scatter(
-        back.reshape(n_m * n_tp, experts * capacity, back_wide),
-        ("m", "tp"),
-        scatter_dimension=0,
-        tiled=False,
+    )(
+        rows,
+        tokens,
+        slot.T,
+        onehot.transpose(1, 2, 0),
+        first[None, :],
+        router_rows,
+        gate_proj,
+        up_proj,
+        down_proj,
     )
 
     tile = 256
@@ -332,31 +583,8 @@
         name="grads",
     )(full, full, d_gate.reshape(total, ff), d_up.reshape(total, ff), scaled.reshape(total, ff))
 
-    home = lax.all_to_all(
-        mine.reshape(experts, capacity, back_wide), "e", split_axis=0, concat_axis=0, tiled=True
-    )
-    route_sum = lax.dot_general(
-        place.reshape(experts * capacity, ntok),
-        home[:, :, :share].reshape(experts * capacity, share),
-        (((0,), (0,)), ((), ())),
-        preferred_element_type=F32,
-    )
-    gate_at = jnp.einsum(
-        "ect,ecl->etl", place, home[:, :, share:], preferred_element_type=F32
-    )[:, :, 0]
-    gate_grad = jnp.sum(onehot * gate_at.T[:, None, :], axis=2)
-    delta = first * (1.0 - first) * (gate_grad[:, 0] - gate_grad[:, 1])
-    dlogits = delta[:, None] * (onehot[:, 0] - onehot[:, 1])
-    router_rows = lax.dynamic_slice_in_dim(router_weight, tp_index * share, share, 0).astype(F32)
-    router_part = lax.dot_general(dlogits, router_rows, NT, precision=lax.Precision.HIGHEST)
-    token_grad = (route_sum + router_part).astype(BF16)
-    n_ep = lax.axis_size("e") * n_m
-    terms = lax.dot_general(
-        dlogits, tokens.astype(F32), (((0,), (0,)), ((), ())), precision=lax.Precision.HIGHEST
-    )
-    terms = terms.reshape(experts, n_ep, width // n_ep).transpose(1, 0, 2)
-    terms = lax.all_to_all(terms, ("e", "m"), split_axis=0, concat_axis=0, tiled=True)
-    router_grad = jnp.sum(terms, axis=0).T
+    gate_grad = gate_rows.T
+    router_grad = router_rows_out[:experts].T
     return (token_grad, gate_grad, router_grad, grad_gate, grad_up, grad_down)
 
 

time: 196 us -> 131 us (0.67)
  waiting for transfers between devices: 74.9 us -> 0 us
  Pallas kernels: 87 us -> 119 us
  between operations: 14.2 us -> 0.71 us
  starting transfers between devices: 8.4 us -> 0 us
  matrix products: 5.82 us -> 3.01 us
  local copies, waits for them, and re-layouts: 2.52 us -> 4.83 us
    reduce_scatter x1 -> x0, waiting for transfers between devices: 65.9 us -> none  [shards(): lax.psum_scatter(back.reshape(n_m * n_tp, experts * capacity, back_wide),...]
    pallas_call x1, Pallas kernels: 72.4 us -> 104 us  [shards(): pl.pallas_call(functools.partial(rows_kernel, share), in_specs=[vmem] * 6...]
    all_to_all x2 -> x0, waiting for transfers between devices: 9.05 us -> none  [the longest x1 5.13 us: shards(): lax.all_to_all(terms, ('e', 'm'), split_axis=0, concat_axis=0, tiled=True)]
    all_to_all x2 -> x0, starting transfers between devices: 8.36 us -> none  [the longest x1 4.59 us: shards(): lax.all_to_all(mine.reshape(experts, capacity, back_wide), 'e', split_axi...]
    dot_general x4 -> x0, matrix products: 2.81 us -> none  [the longest x1 1.16 us: shards(): lax.dot_general(dlogits, router_rows, NT, precision=lax.Precision.HIGHEST)]
  transfers between devices with their start and end apart: 3 -> 0, of which waited for: 3 -> 0; matrix products, arithmetic and copies ran while one was open for 1% -> 0% of each run, Pallas kernels for 8% -> 0%
where the time goes in v1:
time: 131 us
  Pallas kernels  119 us (91%)
  local copies, waits for them, and re-layouts  4.83 us (4%)
  other arithmetic  3.46 us (3%)
  matrix products  3.01 us (2%)
    pallas_call x1, Pallas kernels, shards(): pl.pallas_call(functools.partial(rows_kernel, share), in_specs=[vmem] * 6...  104 us
    pallas_call x1, Pallas kernels, shards(): pl.pallas_call(grads_kernel, grid=(width // tile,), in_specs=[pl.BlockSpe...  14.7 us

profile of v1, /device:TPU:0, one launch (start us, length us, event | category | flops | bytes accessed | tf_op | source)
XLA Modules:
  0.0 130.9 jit_solution(8582461829577982600)
XLA Ops:
  0.6 0.0 copy-start
  0.7 0.7 copy-done
  1.4 1.3 fusion.4
  2.6 0.7 select_reduce_fusion.1
  3.4 0.0 copy-start.4
  3.4 0.1 eq.43
  3.5 0.7 select_reduce_fusion
  4.2 0.1 fusion.slot_ref
  4.3 0.0 copy-start.2
  4.3 1.3 fusion.1.oh_ref
  5.6 0.6 pad_convert_fusion.rw_ref
  6.2 0.1 copy.16
  6.4 0.1 bitcast_compare_fusion
  6.5 1.1 constant_dynamic-slice_fusion
  7.6 0.3 concatenate.8
  7.9 1.6 %convolution_convert_fusion = bf16[320,2176]{1,0:T(8,128)(2,1)} fusion(pred[320,128]{1,0:T(32,128)(4,1)S(1)} %bitcast_compare_fusion, bf16[128,2176]{1,0:T(8,128)(2,1)S(1)} %concatenate.8), kind=kOutput, calls=%fused_computation | convolution fusion | flops 178954240 | bytes 1990656 | tf_op jit(solution)/shard_map/dot_general | solution.py:474
  9.5 0.0 copy-done.4
  9.5 0.0 copy-done.2
  9.5 104.2 %rows.1 = (bf16[4,4,2,80,2176]{4,3,2,1,0:T(8,128)(2,1)}, bf16[4,320,512]{2,1,0:T(8,128)(2,1)}, bf16[4,320,512]{2,1,0:T(8,128)(2,1)}, bf16[4,320,512]{2,1,0:T(8,1...) custom-call(bf16[4,80,2176]{2,1,0:T(8,128)(2,1)} %bitcast.19, bf16[128,2048]{1,0:T(8,128)(2,1)} %tok_ref.1, ...), custom_call_target="tpu_custom_call" | custom-call | flops 13421772800 | bytes 31457280 | tf_op jit(solution)/shard_map/rows/pallas_call | solution.py:493
  113.6 1.3 slice_bitcast_fusion
  114.9 0.0 copy-start.1
  114.9 0.0 copy-start.3
  114.9 14.7 %grads.1 = (f32[1,2048,512]{2,1,0:T(8,128)}, f32[1,2048,512]{2,1,0:T(8,128)}, f32[1,512,2048]{2,1,0:T(8,128)}) custom-call(bf16[4,4,2,80,2176]{4,3,2,1,0:T(8,128)(2,1)} %get-tuple-element.19.x_ref.c_ref, bf16[4,4,2,80,2176]{4,3,2,1,0:T(8,128)(2,1)} %get-tuple-element.19.x_ref.c_ref, bf16[1280,512]{1,0:T(8,128)(2,1)} %bitcast.23, bf16[1280,512]{1,0:T(8,128)(2,1)} %bitcast.24, ...), custom_call_target="tpu_custom_call" | custom-call | flops 8053063680 | bytes 31457280 | tf_op jit(solution)/shard_map/grads/pallas_call | solution.py:561
  129.6 0.0 copy-done.1
  129.6 0.7 copy.21
  130.3 0.0 copy-done.3
  130.3 0.6 copy.22
  (6 shorter events, 0.0 us)
Async XLA Ops:
  0.6 0.7 copy-start
  3.4 6.1 %copy-start.4 = (f32[128,1]{0,1:T(1,128)}, f32[128,1]{0,1:T(1,128)S(1)}, u32[]{:S(2)}) copy-start(f32[128,1]{0,1:T(1,128)S(1)} %get-tuple-element.29) | copy-start | bytes 1540
  4.3 5.2 %copy-start.2 = (s32[4,128]{1,0:T(4,128)}, s32[4,128]{1,0:T(4,128)S(1)}, u32[]{:S(2)}) copy-start(s32[4,128]{1,0:T(4,128)S(1)} %fusion.slot_ref) | copy-start | bytes 6148
  114.9 14.7 %copy-start.1 = (bf16[128,1024]{1,0:T(8,128)(2,1)S(1)}, bf16[128,1024]{1,0:T(8,128)(2,1)}, u32[]{:S(2)}) copy-start(bf16[128,1024]{1,0:T(8,128)(2,1)} %get-tuple-element.38) | copy-start | bytes 786436
  114.9 15.4 %copy-start.3 = (f32[2,128]{1,0:T(2,128)S(1)}, f32[2,128]{1,0:T(2,128)}, u32[]{:S(2)}) copy-start(f32[2,128]{1,0:T(2,128)} %get-tuple-element.17) | copy-start | bytes 3076

commit v2 on v1

--- a/solution.py
+++ b/solution.py
@@ -17,11 +17,11 @@
 
 
 def rows_kernel(
-    share, send_ref, tok_ref, slot_ref, oh_ref, first_ref, rw_ref, wg_hbm, wu_hbm, wd_hbm,
-    x_hbm, dg_hbm, du_hbm, sc_hbm, grad_ref, gate_ref, router_ref,
-    full, wg_ref, wu_ref, wd_ref, dg_ref, du_ref, sc_ref, back, core_in, xa_in, yb_in, ya_in, xb_in, home, place,
+    share, tok_ref, cot_ref, route_ref, rw_ref, wg_hbm, wu_hbm, wd_hbm,
+    gg_ref, gu_ref, gd_ref, grad_ref, gate_ref, router_ref,
+    send_ref, full, wg_ref, wu_ref, wd_ref, dg_ref, du_ref, sc_ref, back, core_in, xa_in, yb_in, ya_in, xb_in, home, place,
     gacc, gcore, gcore_in, gx_in, gt, gz, terms, terms_in,
-    out_sem, hid_sem, send_sem, recv_sem, load_sem, gsend, grecv, tsend, trecv,
+    send_sem, recv_sem, load_sem, gsend, grecv, tsend, trecv,
 ):
     experts, n_m, n_tp, capacity, _ = full.shape
     ntok, width = tok_ref.shape
@@ -53,13 +53,49 @@
         pl.semaphore_signal(barrier, inc=1, device_id=(e, m, ahead(j)), device_id_type=MESH)
     loads = [
         pltpu.make_async_copy(src, dst, load_sem.at[n])
-        for n, (src, dst) in enumerate(
-            [(send_ref.at[e], full.at[0, m, t]), (wg_hbm, wg_ref), (wu_hbm, wu_ref), (wd_hbm, wd_ref)]
-        )
+        for n, (src, dst) in enumerate([(wg_hbm, wg_ref), (wu_hbm, wu_ref), (wd_hbm, wd_ref)])
     ]
     for load in loads:
         load.start()
+
+    logits = lax.dot_general(rw_ref[...], tok_ref[...], NT, preferred_element_type=F32)
+    picks = [
+        [jnp.where(route_ref[n : n + 1, :] == at, 1.0, 0.0) for at in range(experts)] for n in range(TOP)
+    ]
+    chosen = [sum(picks[n][at] * logits[at : at + 1] for at in range(experts)) for n in range(TOP)]
+    first = jax.nn.sigmoid(chosen[0] - chosen[1])
+    used = [gate.astype(BF16).astype(F32) for gate in (first, 1.0 - first)]
+    pad = -experts % 8
+    blank = [jnp.zeros((pad, ntok), F32)] if pad else []
+    named = jnp.concatenate([picks[0][at] + picks[1][at] for at in range(experts)] + blank, axis=0)
+    order = lax.broadcasted_iota(jnp.int32, (ntok, ntok), 0) < lax.broadcasted_iota(jnp.int32, (ntok, ntok), 1)
+    rank = jnp.dot(named.astype(BF16), jnp.where(order, 1.0, 0.0).astype(BF16), preferred_element_type=F32)
+    slot = jnp.where(named > 0.0, rank, -1.0).astype(jnp.int32)
+    line = lax.broadcasted_iota(jnp.int32, (capacity, ntok), 0)
+    for at in range(experts):
+        chosen_slot = jnp.where(line == slot[at : at + 1], 1.0, 0.0)
+        place[at] = chosen_slot.astype(BF16)
+        gate_row = picks[0][at] * used[0] + picks[1][at] * used[1]
+        gate_col = jnp.sum(chosen_slot * gate_row, axis=1, keepdims=True)
+        send_ref[at, :, 2 * share :] = jnp.broadcast_to(gate_col, (capacity, LANES)).astype(BF16)
+    mine_cols = pl.ds(pl.multiple_of(t * share, LANES), share)
+    spots = place[...].reshape(experts * capacity, ntok)
+    for n, ref in enumerate((tok_ref, cot_ref)):
+        rows = jnp.dot(spots, ref[:, mine_cols], preferred_element_type=F32).astype(BF16)
+        send_ref[:, :, n * share : (n + 1) * share] = rows.reshape(experts, capacity, share)
+    keep = pltpu.make_async_copy(send_ref.at[e], full.at[e, m, t], load_sem.at[3])
+    keep.start()
+    for ref in (gacc, gg_ref, gu_ref, gd_ref):
+        ref[...] = jnp.zeros_like(ref)
     pl.semaphore_wait(barrier, n_ep - 1 + n_tp - 1)
+
+    near = lax.min(e, experts - 1 - e)
+    side = 1 - 2 * lax.div(2 * e, experts)
+
+    def source(i):
+        step, both = lax.div(i + 1, 2), i <= 2 * near
+        away = jnp.where(both, step, i - near)
+        return e + side * jnp.where(both & (lax.rem(i, 2) == 0), -away, away)
 
     def remote(src, dst, kind, k, device):
         return pltpu.make_async_remote_copy(
@@ -97,13 +133,10 @@
     def sent(ref, kind, k):
         remote(ref, ref, kind, k, core_to).wait_send()
 
-    for k in range(1, experts):
-        there = lax.rem(e + k, experts)
-        remote(send_ref.at[there], full.at[k, m, t], Z, k, (there, m, t)).start()
-
-    def own(k):
+    def own(k, away):
         mine = piece(k, m, t)
-        @pl.when(k > 0)
+
+        @pl.when(away)
         def _():
             landed(mine, Z, k)
             pass_on(mine, X, k, x_to)
@@ -111,13 +144,13 @@
                 pass_on(mine, y_kind(j), k, (e, m, ahead(j)))
             pass_on(mine, CORE_OWN, k, core_to)
 
-        @pl.when(k == 0)
+        @pl.when(jnp.logical_not(away))
         def _():
             src = send_ref.at[e]
-            remote(src, mine, X, 0, x_to).start()
+            remote(src, mine, X, k, x_to).start()
             for j in range(1, n_tp):
-                remote(src, mine, y_kind(j), 0, (e, m, ahead(j))).start()
-            remote(src, mine, CORE_OWN, 0, core_to).start()
+                remote(src, mine, y_kind(j), k, (e, m, ahead(j))).start()
+            remote(src, mine, CORE_OWN, k, core_to).start()
 
     def neighbours(k):
         across = piece(k, x_peer, t)
@@ -147,13 +180,10 @@
             landed(piece(k, core_peer, behind(j)), core_y(j), k)
             landed(piece(k, other_x, behind(j), first_cols), core_a(j), k)
             landed(piece(k, other_x, behind(j), last_cols), core_b(j), k)
-        pltpu.make_async_copy(full.at[k], x_hbm.at[k], out_sem.at[k]).start()
-
-    def hidden_copies(k):
-        pairs = ((dg_ref, dg_hbm), (du_ref, du_hbm), (sc_ref, sc_hbm))
-        return [pltpu.make_async_copy(a.at[k], b.at[k], hid_sem.at[n, k]) for n, (a, b) in enumerate(pairs)]
-
-    def compute(k):
+
+    def compute(n):
+        k = source(n)
+
         def part(tp_at, base, size):
             return full[k, :, tp_at, :, base : base + size].reshape(held, size)
 
@@ -174,7 +204,7 @@
         qvals = contract(share, wd_ref, True)
         extra = part(0, 2 * share, LANES).astype(F32)
         lane = lax.broadcasted_iota(jnp.int32, extra.shape, 1)
-        weight = jnp.sum(jnp.where(lane == e, extra, 0.0), axis=1, keepdims=True)
+        weight = extra[:, :1]
         sig = jax.nn.sigmoid(gpre)
         silu_val = gpre * sig
         hidden = (silu_val * upre).astype(BF16).astype(F32)
@@ -182,13 +212,10 @@
         dhid = weight * qvals
         d_gate = (dhid * upre * sig * (1.0 + gpre * (1.0 - sig))).astype(BF16)
         d_up = (dhid * silu_val).astype(BF16)
-        dg_ref[k] = d_gate
-        du_ref[k] = d_up
-        sc_ref[k] = (weight * hidden).astype(BF16)
-        for copy in hidden_copies(k):
-            copy.start()
-        source = lax.rem(e + experts - k, experts)
-        gate_lanes = jnp.where(lane == source, gate_part, 0.0).reshape(n_m, capacity, LANES)
+        dg_ref[n] = d_gate
+        du_ref[n] = d_up
+        sc_ref[n] = (weight * hidden).astype(BF16)
+        gate_lanes = jnp.where(lane == k, gate_part, 0.0).reshape(n_m, capacity, LANES)
         for at in range(n_m):
             gacc[at % 2, at // 2, :capacity, :] += gate_lanes[at]
         for tp_at in range(n_tp):
@@ -200,6 +227,26 @@
                 back[k, at % 2, at // 2, tp_at] = grad[at]
         remote(back.at[k, 1 - core], core_in.at[k], R1, k, core_to).start()
 
+    group = 2 - experts % 2
+
+    def weight_grads(n, part):
+        tp_at, down = part // 2, part % 2
+        cols = slice(tp_at * share, (tp_at + 1) * share)
+
+        def rows(base):
+            parts = [full[source(n + g), :, tp_at, :, base : base + share] for g in range(group)]
+            return jnp.concatenate([at.reshape(held, share) for at in parts], axis=0)
+
+        def units(ref):
+            return ref[pl.ds(n, group)].reshape(group * held, -1)
+
+        if down:
+            gd_ref[0, :, cols] += jnp.dot(units(sc_ref).T, rows(share), preferred_element_type=F32)
+        else:
+            flipped = rows(0).T
+            gg_ref[0, cols, :] += jnp.dot(flipped, units(dg_ref), preferred_element_type=F32)
+            gu_ref[0, cols, :] += jnp.dot(flipped, units(du_ref), preferred_element_type=F32)
+
     def add(*terms):
         total = terms[0].astype(F32)
         for term in terms[1:]:
@@ -248,38 +295,64 @@
         ref[:, :half] = add(ref[:, :half], xa_in[k, t], *[ya_in[k, j - 1] for j in range(1, n_tp)])
         ref[:, half:] = add(ref[:, half:], xb_in[k], *[yb_in[k, j - 1, x_half] for j in range(1, n_tp)])
 
-        def away():
-            there = lax.rem(e + experts - k, experts)
-            remote(ref, home.at[e], RET, k, (there, m, t)).start()
-
-        def here():
+        @pl.when(k != e)
+        def _():
+            ret_copy(k, e).start()
+
+        @pl.when(k == e)
+        def _():
             home[e] = ref[...]
 
-        if isinstance(k, int):
-            (away if k else here)()
-        else:
-            pl.when(k > 0)(away)
-            pl.when(k == 0)(here)
-
-    gacc[...] = jnp.zeros_like(gacc)
+    def ret_copy(k, at):
+        return pltpu.make_async_remote_copy(
+            src_ref=mine_back(k),
+            dst_ref=home.at[at],
+            send_sem=send_sem.at[RET, k],
+            recv_sem=recv_sem.at[RET, at],
+            device_id=(k, m, t),
+            device_id_type=MESH,
+        )
+
+    def send_z(i, carry):
+        there = source(i)
+        z_copy(there, e).start()
+        return carry
+
+    def z_copy(there, at):
+        return pltpu.make_async_remote_copy(
+            src_ref=send_ref.at[there],
+            dst_ref=full.at[at, m, t],
+            send_sem=send_sem.at[Z, there],
+            recv_sem=recv_sem.at[Z, at],
+            device_id=(there, m, t),
+            device_id_type=MESH,
+        )
+
+    lax.fori_loop(1, experts, send_z, 0)
 
     def step(i, carry):
-        pl.when(i < experts)(lambda: own(i))
-        pl.when((i >= 1) & (i < experts + 1))(lambda: neighbours(i - 1))
-        pl.when(i >= 3)(lambda: reduce_first(i - 3))
-        pl.when(i >= 4)(lambda: reduce_second(i - 4))
-        pl.when(i >= 5)(lambda: reduce_third(i - 5))
+        pl.when((i >= 1) & (i < experts + 1))(lambda: neighbours(source(i - 1)))
+        pl.when(i >= 2)(lambda: corners(source(i - 2)))
+        pl.when(i < experts)(lambda: own(source(i), i > 0))
+        pl.when(i >= 3)(lambda: reduce_first(source(i - 3)))
+        pl.when(i >= 4)(lambda: reduce_second(source(i - 4)))
+        pl.when(i >= 5)(lambda: reduce_third(source(i - 5)))
 
         @pl.when(i == 2)
         def _():
+            keep.wait()
             for load in loads:
                 load.wait()
 
         @pl.when(i >= 2)
         def _():
-            corners(i - 2)
-            partner(i - 2)
+            partner(source(i - 2))
             compute(i - 2)
+
+        @pl.when((i >= 1 + group) & (lax.rem(i - 1, group) == 0) & (i < experts + 1))
+        def _():
+            for part in range(2 * n_tp):
+                weight_grads(i - 1 - group, part)
 
         return carry
 
@@ -296,25 +369,30 @@
         )
 
     erows = gcore.shape[2]
-    last = experts - 1
+    last, second, third = [source(experts - n) for n in (1, 2, 3)]
     for at in range(n_m):
         gcore[at % 2, at // 2] = gacc[at % 2, at // 2].T[:erows]
     to_core = gate_copy(gcore.at[1 - core], gcore_in, 0, core_to)
     to_core.start()
     reduce_first(last)
+    rest = [functools.partial(weight_grads, experts - group, part) for part in range(2 * n_tp)]
+    rest.pop()()
     to_core.wait_recv()
     gcore[core] = gcore[core] + gcore_in[...]
     to_x = gate_copy(gcore.at[core, x_other], gx_in, 1, x_to)
     to_x.start()
-    reduce_second(last - 1)
-    reduce_third(last - 2)
+    reduce_second(second)
+    reduce_third(third)
+    rest.pop()()
     to_x.wait_recv()
     gt[t] = gcore[core, x_half] + gx_in[...]
     to_t = [gate_copy(gt.at[t], gt.at[t], 1 + j, (e, m, ahead(j))) for j in range(1, n_tp)]
     for copy in to_t:
         copy.start()
     reduce_second(last)
-    reduce_third(last - 1)
+    reduce_third(second)
+    for part in rest:
+        part()
     for j in range(1, n_tp):
         gate_copy(gt.at[behind(j)], gt.at[behind(j)], 1 + j, (e, m, ahead(j))).wait_recv()
     whole = gt[0]
@@ -326,10 +404,6 @@
     ]
     for copy in to_z:
         copy.start()
-    for at in range(experts):
-        rows = lax.broadcasted_iota(jnp.int32, (capacity, ntok), 0)
-        place[at] = jnp.where(rows == slot_ref[at : at + 1, :], 1.0, 0.0).astype(BF16)
-    reduce_third(last)
     for k in range(1, experts):
         src = gz.at[lax.rem(e + experts - k, experts)]
         gate_copy(src, src, n_tp + k, core_to).wait_recv()
@@ -342,15 +416,11 @@
         line = jnp.broadcast_to(line, (8, LANES))[:, :capacity]
         got = jnp.dot(line, place[at].astype(F32), precision=HIGHEST, preferred_element_type=F32)
         gates.append(got[0:1])
-    picks = [[oh_ref[n, at : at + 1, :] for at in range(experts)] for n in range(TOP)]
     gate = [sum(picks[n][at] * gates[at] for at in range(experts)) for n in range(TOP)]
-    first = first_ref[...]
     delta = first * (1.0 - first) * (gate[0] - gate[1])
     gate_ref[0:1] = gate[0]
     gate_ref[1:2] = gate[1]
-    pad = -experts % 8
-    zero = [jnp.zeros((pad, ntok), F32)] if pad else []
-    dlog = jnp.concatenate([delta * (picks[0][at] - picks[1][at]) for at in range(experts)] + zero, axis=0)
+    dlog = jnp.concatenate([delta * (picks[0][at] - picks[1][at]) for at in range(experts)] + blank, axis=0)
     term = jnp.dot(dlog, tok_ref[...].astype(F32), precision=HIGHEST, preferred_element_type=F32)
     cols = width // n_ep
     for at in range(n_ep):
@@ -373,12 +443,15 @@
 
     lax.fori_loop(1, n_ep, each, 0)
 
+    reduce_third(last)
+    weight_rows = [rw_ref[:, mine_cols].astype(F32)] + ([jnp.zeros((pad, share), F32)] if pad else [])
     router_part = lax.dot_general(
-        dlog, rw_ref[...], (((0,), (0,)), ((), ())), precision=HIGHEST, preferred_element_type=F32
+        dlog, jnp.concatenate(weight_rows, axis=0), (((0,), (0,)), ((), ())), precision=HIGHEST, preferred_element_type=F32
     )
     spread = place[...].reshape(experts * capacity, ntok).T
     for k in range(1, experts):
-        landed(home.at[lax.rem(e + k, experts)], RET, k)
+        at = lax.rem(e + k, experts)
+        ret_copy(at, at).wait_recv()
     route_sum = jnp.dot(spread, home[...].reshape(experts * capacity, share), preferred_element_type=F32)
     grad_ref[...] = (route_sum + router_part).astype(BF16)
 
@@ -386,7 +459,7 @@
         term_copy(d).wait_recv()
         return total + terms_in[d, :, :cols]
 
-    router_ref[...] = lax.fori_loop(1, n_ep, gather, terms[me, :, :cols])
+    router_ref[...] = lax.fori_loop(1, n_ep, gather, terms[me, :, :cols])[:experts]
 
     def done(d, carry):
         term_copy(d).wait_send()
@@ -398,10 +471,12 @@
 
     def finish(k, carry):
         mine = piece(k, m, t)
-        @pl.when(k > 0)
+
+        @pl.when(k != e)
         def _():
             sent(mine, Z, k)
             sent(mine_back(k), RET, k)
+
         sent(mine, X, k)
         sent(mine, CORE_OWN, k)
         sent(piece(k, x_peer, t), CORE_X, k)
@@ -417,25 +492,21 @@
             sent(piece(k, x_peer, behind(j), last_cols), core_b(j), k)
             sent(across_b(k, j), r2b(j), k)
             sent(onward_a(k, j), r3a(j), k)
-        pltpu.make_async_copy(full.at[k], x_hbm.at[k], out_sem.at[k]).wait()
-        for copy in hidden_copies(k):
-            copy.wait()
         return carry
 
     lax.fori_loop(0, experts, finish, 0)
 
 
-def grads_kernel(x_ref, c_ref, dg_ref, du_ref, sc_ref, gg_ref, gu_ref, gd_ref, sct):
-    @pl.when(pl.program_id(0) == 0)
-    def _():
-        sct[...] = sc_ref[...].T
-
-    tile = x_ref.shape[-1]
-    rows = dg_ref.shape[0]
-    xt = x_ref[:, :, 0].reshape(rows, tile).T
-    gg_ref[0] = jnp.dot(xt, dg_ref[...], preferred_element_type=F32)
-    gu_ref[0] = jnp.dot(xt, du_ref[...], preferred_element_type=F32)
-    gd_ref[0] = jnp.dot(sct[...], c_ref[:, :, 0].reshape(rows, tile), preferred_element_type=F32)
+def hand_over(*refs):
+    n = len(refs) // 2
+    copies = [
+        pltpu.make_async_copy(src, dst, refs[-1].at[at])
+        for at, (src, dst) in enumerate(zip(refs[:n], refs[n:-1]))
+    ]
+    for copy in copies:
+        copy.start()
+    for copy in copies:
+        copy.wait()
 
 
 def shards(tokens, routes, router_weight, gate_proj, up_proj, down_proj, cotangent):
@@ -445,38 +516,9 @@
     share = width // n_tp
     capacity = min(ntok, 5 * TOP * ntok // (4 * experts))
     capacity = -(-capacity // 16) * 16
-    tp_index = lax.axis_index("tp")
     ff = gate_proj.shape[2]
 
-    logits = jnp.dot(tokens, router_weight, preferred_element_type=F32)
-    onehot = (routes[:, :, None] == jnp.arange(experts, dtype=jnp.int32)[None, None, :]).astype(F32)
-    chosen = jnp.sum(onehot * logits[:, None, :], axis=2)
-    first = jax.nn.sigmoid(chosen[:, 0] - chosen[:, 1])
-    gates = jnp.stack([first, 1.0 - first], axis=1)
-    used = gates.astype(BF16)
-    named = jnp.sum(onehot, axis=1)
-    below = (jnp.arange(ntok)[:, None] > jnp.arange(ntok)[None, :]).astype(BF16)
-    rank = jnp.dot(below, named.astype(BF16), preferred_element_type=F32)
-    slot = jnp.where(named > 0, rank, -1.0).astype(jnp.int32)
-    place = (
-        jnp.arange(capacity, dtype=jnp.int32)[None, :, None] == slot.T[:, None, :]
-    ).astype(BF16)
-    gate_cols = jnp.sum(onehot * used.astype(F32)[:, :, None], axis=1).astype(BF16)
-    payload = jnp.concatenate(
-        [
-            lax.dynamic_slice_in_dim(tokens, tp_index * share, share, 1),
-            lax.dynamic_slice_in_dim(cotangent, tp_index * share, share, 1),
-            gate_cols,
-            jnp.zeros((ntok, LANES - experts), BF16),
-        ],
-        axis=1,
-    )
-    rows = jnp.dot(
-        place.reshape(experts * capacity, ntok), payload, preferred_element_type=F32
-    ).astype(BF16)
     wide = 2 * share + LANES
-    rows = rows.reshape(experts, capacity, wide)
-
     held = n_m * capacity
     hid_shape = jax.ShapeDtypeStruct((experts, held, ff), BF16)
     flops = 2 * experts * held * width * ff
@@ -485,25 +527,23 @@
     half = share // 2
     erows = -(-experts // 8) * 8
     cols = width // n_ep
-    router_rows = lax.dynamic_slice_in_dim(router_weight, tp_index * share, share, 0).astype(F32).T
-    router_rows = jnp.pad(router_rows, ((0, erows - experts), (0, 0)))
     vmem = pl.BlockSpec(memory_space=pltpu.VMEM)
     anywhere = pl.BlockSpec(memory_space=pl.ANY)
     full_shape = (experts, n_m, n_tp, capacity, wide)
-    full, d_gate, d_up, scaled, token_grad, gate_rows, router_rows_out = pl.pallas_call(
+    grad_gate, grad_up, grad_down, token_grad, gate_rows, router_rows = pl.pallas_call(
         functools.partial(rows_kernel, share),
-        in_specs=[vmem] * 6 + [anywhere] * 3,
-        out_specs=[anywhere] * 4 + [vmem] * 3,
+        in_specs=[vmem] * 4 + [anywhere] * 3,
+        out_specs=[vmem] * 6,
         out_shape=[
-            jax.ShapeDtypeStruct(full_shape, BF16),
-            hid_shape,
-            hid_shape,
-            hid_shape,
-            jax.ShapeDtypeStruct((ntok, share), BF16),
-            jax.ShapeDtypeStruct((TOP, ntok), F32),
-            jax.ShapeDtypeStruct((erows, cols), F32),
+            pltpu.VMEM(gate_proj.shape, F32),
+            pltpu.VMEM(up_proj.shape, F32),
+            pltpu.VMEM(down_proj.shape, F32),
+            pltpu.VMEM((ntok, share), BF16),
+            pltpu.VMEM((TOP, ntok), F32),
+            pltpu.VMEM((experts, cols), F32),
         ],
         scratch_shapes=[
+            pltpu.VMEM((experts, capacity, wide), BF16),
             pltpu.VMEM(full_shape, BF16),
             pltpu.VMEM(gate_proj.shape, BF16),
             pltpu.VMEM(up_proj.shape, BF16),
@@ -527,8 +567,6 @@
             pltpu.VMEM((experts, erows, LANES), F32),
             pltpu.VMEM((n_ep, erows, LANES), F32),
             pltpu.VMEM((n_ep, erows, LANES), F32),
-            pltpu.SemaphoreType.DMA((experts,)),
-            pltpu.SemaphoreType.DMA((3, experts)),
             pltpu.SemaphoreType.DMA((kinds, experts)),
             pltpu.SemaphoreType.DMA((kinds, experts)),
             pltpu.SemaphoreType.DMA((4,)),
@@ -538,54 +576,31 @@
             pltpu.SemaphoreType.DMA((n_ep,)),
         ],
         compiler_params=pltpu.CompilerParams(
-            collective_id=0, has_side_effects=True, vmem_limit_bytes=60 << 20
+            collective_id=0, has_side_effects=True, vmem_limit_bytes=46 << 20
         ),
         cost_estimate=pl.CostEstimate(flops=5 * flops, bytes_accessed=30 << 20, transcendentals=0),
         name="rows",
     )(
-        rows,
         tokens,
-        slot.T,
-        onehot.transpose(1, 2, 0),
-        first[None, :],
-        router_rows,
+        cotangent,
+        routes.T,
+        router_weight.T,
         gate_proj,
         up_proj,
         down_proj,
     )
 
-    tile = 256
-    per = share // tile
-    total = experts * held
-    whole = lambda i: (0, 0)
-    grad_gate, grad_up, grad_down = pl.pallas_call(
-        grads_kernel,
-        grid=(width // tile,),
-        in_specs=[
-            pl.BlockSpec((experts, n_m, 1, capacity, tile), lambda i: (0, 0, i // per, 0, i % per)),
-            pl.BlockSpec((experts, n_m, 1, capacity, tile), lambda i: (0, 0, i // per, 0, per + i % per)),
-            pl.BlockSpec((total, ff), whole),
-            pl.BlockSpec((total, ff), whole),
-            pl.BlockSpec((total, ff), whole),
-        ],
-        out_specs=[
-            pl.BlockSpec((1, tile, ff), lambda i: (0, i, 0)),
-            pl.BlockSpec((1, tile, ff), lambda i: (0, i, 0)),
-            pl.BlockSpec((1, ff, tile), lambda i: (0, 0, i)),
-        ],
-        out_shape=[
-            jax.ShapeDtypeStruct(gate_proj.shape, F32),
-            jax.ShapeDtypeStruct(up_proj.shape, F32),
-            jax.ShapeDtypeStruct(down_proj.shape, F32),
-        ],
-        scratch_shapes=[pltpu.VMEM((ff, total), BF16)],
-        cost_estimate=pl.CostEstimate(flops=3 * flops, bytes_accessed=30 << 20, transcendentals=0),
-        name="grads",
-    )(full, full, d_gate.reshape(total, ff), d_up.reshape(total, ff), scaled.reshape(total, ff))
-
-    gate_grad = gate_rows.T
-    router_grad = router_rows_out[:experts].T
-    return (token_grad, gate_grad, router_grad, grad_gate, grad_up, grad_down)
+    results = (grad_gate, grad_up, grad_down, token_grad, gate_rows, router_rows)
+    grad_gate, grad_up, grad_down, token_grad, gate_rows, router_rows = pl.pallas_call(
+        hand_over,
+        in_specs=[vmem] * 6,
+        out_specs=[anywhere] * 6,
+        out_shape=[jax.ShapeDtypeStruct(at.shape, at.dtype) for at in results],
+        scratch_shapes=[pltpu.SemaphoreType.DMA((6,))],
+        compiler_params=pltpu.CompilerParams(vmem_limit_bytes=1 << 20),
+        name="hand_over",
+    )(*results)
+    return (token_grad, gate_rows.T, router_rows.T, grad_gate, grad_up, grad_down)
 
 
 def solution(mesh):

time: 131 us -> 111 us (0.85)
  Pallas kernels: 119 us -> 110 us
  local copies, waits for them, and re-layouts: 4.83 us -> 0 us
  other arithmetic: 3.46 us -> 0 us
  matrix products: 3.01 us -> 0 us
    pallas_call x2, Pallas kernels: 119 us -> 110 us  [the longest x1 105 us: shards(): pl.pallas_call(functools.partial(rows_kernel, share), in_specs=[vmem] * 4...]
    dot_general x3 -> x0, matrix products: 3.01 us -> none  [the longest x1 1.6 us: shards(): jnp.dot(place.reshape(experts * capacity, ntok), payload, preferred_eleme...]
    unnamed x12 -> x0, local copies, waits for them, and re-layouts: 1.99 us -> none
    reduce_sum x2 -> x0, other arithmetic: 1.41 us -> none  [the longest x1 0.71 us: shards(): chosen = jnp.sum(onehot * logits[:, None, :], axis=2)]
where the time goes in v2:
time: 111 us
  Pallas kernels  110 us (99%)
    pallas_call x1, Pallas kernels, shards(): pl.pallas_call(functools.partial(rows_kernel, share), in_specs=[vmem] * 4...  105 us
    pallas_call x1, Pallas kernels, shards(): pl.pallas_call(hand_over, in_specs=[vmem] * 6, out_specs=[anywhere] * 6,...  4.72 us

profile of v2, /device:TPU:0, one launch (start us, length us, event | category | flops | bytes accessed | tf_op | source)
XLA Modules:
  0.0 110.7 jit_solution(9906526509578391973)
XLA Ops:
  0.6 105.1 %rows.1 = (f32[1,2048,512]{2,1,0:T(8,128)S(1)}, f32[1,2048,512]{2,1,0:T(8,128)S(1)}, f32[1,512,2048]{2,1,0:T(8,128)S(1)}, bf16[128,1024]{1,0:T(8,128)(2,1)S(1)},...) custom-call(bf16[128,2048]{1,0:T(8,128)(2,1)} %tok_ref.1, bf16[128,2048]{1,0:T(8,128)(2,1)} %cot_ref.1, s32[2,128]{1,0:T(2,128)} %bitcast.6, ...), custom_call_target="tpu_custom_call" | custom-call | flops 13421772800 | bytes 31457280 | tf_op jit(solution)/shard_map/rows/pallas_call | solution.py:533
  105.8 4.7 %hand_over.1 = (f32[1,2048,512]{2,1,0:T(8,128)}, f32[1,2048,512]{2,1,0:T(8,128)}, f32[1,512,2048]{2,1,0:T(8,128)}, bf16[128,1024]{1,0:T(8,128)(2,1)}, f32[2,128]{1,0:T(2,128)}, /*index=5*/f32[4,128]{1,0:T(4,128)}) custom-call(f32[1,2048,512]{2,1,0:T(8,128)S(1)} %get-tuple-element.18.refs_0_, f32[1,2048,512]{2,1,0:T(8,128)S(1)} %get-tuple-element.19.refs_1_, ...), custom_call_target="tpu_custom_call" | custom-call | tf_op jit(solution)/shard_map/hand_over/pallas_call | solution.py:594

commit v3 on v2

--- a/solution.py
+++ b/solution.py
@@ -19,9 +19,9 @@
 def rows_kernel(
     share, tok_ref, cot_ref, route_ref, rw_ref, wg_hbm, wu_hbm, wd_hbm,
     gg_ref, gu_ref, gd_ref, grad_ref, gate_ref, router_ref,
-    send_ref, full, wg_ref, wu_ref, wd_ref, dg_ref, du_ref, sc_ref, back, core_in, xa_in, yb_in, ya_in, xb_in, home, place,
+    send_ref, gw, gw_in, full, wg_ref, wu_ref, wd_ref, dg_ref, du_ref, sc_ref, back, core_in, xa_in, yb_in, ya_in, xb_in, home, place,
     gacc, gcore, gcore_in, gx_in, gt, gz, terms, terms_in,
-    send_sem, recv_sem, load_sem, gsend, grecv, tsend, trecv,
+    send_sem, recv_sem, load_sem, gsend, grecv, tsend, trecv, wsend, wrecv,
 ):
     experts, n_m, n_tp, capacity, _ = full.shape
     ntok, width = tok_ref.shape
@@ -33,7 +33,7 @@
     x_peer = lax.rem(m + 2, 4)
     core_peer = m + 1 - 2 * core
     held = n_m * capacity
-    first_cols, last_cols = pl.ds(0, share), pl.ds(share, share + LANES)
+    first_cols, last_cols = pl.ds(0, share), pl.ds(share, share)
     low, high = pl.ds(0, half), pl.ds(half, share - half)
 
     def ahead(j):
@@ -75,18 +75,22 @@
     for at in range(experts):
         chosen_slot = jnp.where(line == slot[at : at + 1], 1.0, 0.0)
         place[at] = chosen_slot.astype(BF16)
-        gate_row = picks[0][at] * used[0] + picks[1][at] * used[1]
-        gate_col = jnp.sum(chosen_slot * gate_row, axis=1, keepdims=True)
-        send_ref[at, :, 2 * share :] = jnp.broadcast_to(gate_col, (capacity, LANES)).astype(BF16)
+        gate_row = (picks[0][at] * used[0] + picks[1][at] * used[1]).astype(BF16)
+        gw[at, :, :capacity] = lax.dot_general(
+            jnp.broadcast_to(gate_row, (8, ntok)), place[at], NT, preferred_element_type=F32
+        )
+    gw_in[me] = gw[e]
     mine_cols = pl.ds(pl.multiple_of(t * share, LANES), share)
     spots = place[...].reshape(experts * capacity, ntok)
     for n, ref in enumerate((tok_ref, cot_ref)):
         rows = jnp.dot(spots, ref[:, mine_cols], preferred_element_type=F32).astype(BF16)
         send_ref[:, :, n * share : (n + 1) * share] = rows.reshape(experts, capacity, share)
-    keep = pltpu.make_async_copy(send_ref.at[e], full.at[e, m, t], load_sem.at[3])
-    keep.start()
-    for ref in (gacc, gg_ref, gu_ref, gd_ref):
-        ref[...] = jnp.zeros_like(ref)
+    for tp_at in range(n_tp):
+        cols = slice(tp_at * share, (tp_at + 1) * share)
+        for n, ref in enumerate((tok_ref, cot_ref)):
+            rows = jnp.dot(place[e], ref[:, cols], preferred_element_type=F32)
+            full[e, m, tp_at, :, n * share : (n + 1) * share] = rows.astype(BF16)
+    gacc[...] = jnp.zeros_like(gacc)
     pl.semaphore_wait(barrier, n_ep - 1 + n_tp - 1)
 
     near = lax.min(e, experts - 1 - e)
@@ -112,15 +116,17 @@
         return ref if cols is None else ref.at[:, cols]
 
     others = n_tp - 1
-    X, CORE_OWN, CORE_X, Z, R1, R2A, R3B, RET = range(8)
-    def y_kind(j): return 8 + (j - 1)
-    def a_kind(j): return 8 + others + (j - 1)
-    def b_kind(j): return 8 + 2 * others + (j - 1)
-    def core_y(j): return 8 + 3 * others + (j - 1)
-    def core_a(j): return 8 + 4 * others + (j - 1)
-    def core_b(j): return 8 + 5 * others + (j - 1)
-    def r2b(j): return 8 + 6 * others + (j - 1)
-    def r3a(j): return 8 + 7 * others + (j - 1)
+    X, CORE_OWN, CORE_X, Z, R1, R2A, R3B, RET = 0, 2, 4, 6, 8, 9, 10, 11
+    def y_kind(j): return 12 + 2 * (j - 1)
+    def core_y(j): return 12 + 2 * others + 2 * (j - 1)
+    def a_kind(j): return 12 + 4 * others + (j - 1)
+    def b_kind(j): return 12 + 5 * others + (j - 1)
+    def core_a(j): return 12 + 6 * others + (j - 1)
+    def core_b(j): return 12 + 7 * others + (j - 1)
+    def r2b(j): return 12 + 8 * others + (j - 1)
+    def r3a(j): return 12 + 9 * others + (j - 1)
+
+    parts = (first_cols, last_cols)
 
     x_to, core_to = (e, x_peer, t), (e, core_peer, t)
 
@@ -133,36 +139,34 @@
     def sent(ref, kind, k):
         remote(ref, ref, kind, k, core_to).wait_send()
 
-    def own(k, away):
-        mine = piece(k, m, t)
-
-        @pl.when(away)
-        def _():
-            landed(mine, Z, k)
-            pass_on(mine, X, k, x_to)
+    def own(k, h):
+        mine = piece(k, m, t, parts[h])
+        landed(mine, Z + h, k)
+        pass_on(mine, X + h, k, x_to)
+        for j in range(1, n_tp):
+            pass_on(mine, y_kind(j) + h, k, (e, m, ahead(j)))
+        pass_on(mine, CORE_OWN + h, k, core_to)
+
+    def neighbours(k, h):
+        across = piece(k, x_peer, t, parts[h])
+
+        def along_y():
             for j in range(1, n_tp):
-                pass_on(mine, y_kind(j), k, (e, m, ahead(j)))
-            pass_on(mine, CORE_OWN, k, core_to)
-
-        @pl.when(jnp.logical_not(away))
-        def _():
-            src = send_ref.at[e]
-            remote(src, mine, X, k, x_to).start()
+                beside = piece(k, m, behind(j), parts[h])
+                landed(beside, y_kind(j) + h, k)
+                if h == 0:
+                    pass_on(beside, a_kind(j), k, x_to)
+                pass_on(beside, core_y(j) + h, k, core_to)
+
+        if h == 0:
+            along_y()
+        landed(across, X + h, k)
+        if h == 1:
             for j in range(1, n_tp):
-                remote(src, mine, y_kind(j), k, (e, m, ahead(j))).start()
-            remote(src, mine, CORE_OWN, k, core_to).start()
-
-    def neighbours(k):
-        across = piece(k, x_peer, t)
-        landed(across, X, k)
-        for j in range(1, n_tp):
-            pass_on(piece(k, x_peer, t, last_cols), b_kind(j), k, (e, m, ahead(j)))
-        pass_on(across, CORE_X, k, core_to)
-        for j in range(1, n_tp):
-            beside = piece(k, m, behind(j))
-            landed(beside, y_kind(j), k)
-            pass_on(piece(k, m, behind(j), first_cols), a_kind(j), k, x_to)
-            pass_on(beside, core_y(j), k, core_to)
+                pass_on(across, b_kind(j), k, (e, m, ahead(j)))
+        pass_on(across, CORE_X + h, k, core_to)
+        if h == 1:
+            along_y()
 
     def corners(k):
         for j in range(1, n_tp):
@@ -171,19 +175,66 @@
                 landed(ref, kind(j), k)
                 pass_on(ref, across(j), k, core_to)
 
+    def own_here():
+        pass_on(piece(e, m, t), X, e, x_to)
+        for j in range(1, n_tp):
+            pass_on(piece(e, m, ahead(j), first_cols), a_kind(j), e, x_to)
+        pass_on(full.at[e, m], CORE_OWN, e, core_to)
+
+    def neighbours_here():
+        across = piece(e, x_peer, t)
+        landed(across, X, e)
+        for j in range(1, n_tp):
+            pass_on(piece(e, x_peer, t, last_cols), b_kind(j), e, (e, m, ahead(j)))
+        pass_on(across, CORE_X, e, core_to)
+
+    def corners_here():
+        for j in range(1, n_tp):
+            ref = piece(e, x_peer, ahead(j), first_cols)
+            landed(ref, a_kind(j), e)
+            pass_on(ref, core_a(j), e, core_to)
+            ref = piece(e, x_peer, behind(j), last_cols)
+            landed(ref, b_kind(j), e)
+            pass_on(ref, core_b(j), e, core_to)
+
     other_x = lax.rem(core_peer + 2, 4)
 
+    def partner_here():
+        landed(full.at[e, core_peer], CORE_OWN, e)
+        landed(piece(e, other_x, t), CORE_X, e)
+        for j in range(1, n_tp):
+            landed(piece(e, other_x, ahead(j), first_cols), core_a(j), e)
+            landed(piece(e, other_x, behind(j), last_cols), core_b(j), e)
+
+    def weight_copy(d):
+        there = ep_at(d)
+        return pltpu.make_async_remote_copy(
+            src_ref=gw.at[there[0]],
+            dst_ref=gw_in.at[me],
+            send_sem=wsend.at[d],
+            recv_sem=wrecv.at[d],
+            device_id=there,
+            device_id_type=MESH,
+        )
+
+    def weights(k):
+        for at in range(n_m):
+            d = lax.rem(me + n_ep - k * n_m - at, n_ep)
+            pl.when(d > 0)(lambda d=d: weight_copy(d).wait_recv())
+        lines = gw_in[pl.ds(k * n_m, n_m)].reshape(n_m * 8, LANES).T
+        return jnp.concatenate([lines[:capacity, 8 * at : 8 * at + 1] for at in range(n_m)], axis=0)
+
     def partner(k):
-        landed(piece(k, core_peer, t), CORE_OWN, k)
-        landed(piece(k, other_x, t), CORE_X, k)
-        for j in range(1, n_tp):
-            landed(piece(k, core_peer, behind(j)), core_y(j), k)
+        for h, cols in enumerate(parts):
+            landed(piece(k, core_peer, t, cols), CORE_OWN + h, k)
+            landed(piece(k, other_x, t, cols), CORE_X + h, k)
+        for j in range(1, n_tp):
+            for h, cols in enumerate(parts):
+                landed(piece(k, core_peer, behind(j), cols), core_y(j) + h, k)
             landed(piece(k, other_x, behind(j), first_cols), core_a(j), k)
             landed(piece(k, other_x, behind(j), last_cols), core_b(j), k)
 
-    def compute(n):
-        k = source(n)
-
+    def compute(k):
         def part(tp_at, base, size):
             return full[k, :, tp_at, :, base : base + size].reshape(held, size)
 
@@ -202,9 +253,8 @@
         gpre = contract(0, wg_ref, False)
         upre = contract(0, wu_ref, False)
         qvals = contract(share, wd_ref, True)
-        extra = part(0, 2 * share, LANES).astype(F32)
-        lane = lax.broadcasted_iota(jnp.int32, extra.shape, 1)
-        weight = extra[:, :1]
+        lane = lax.broadcasted_iota(jnp.int32, (held, LANES), 1)
+        weight = weights(k)
         sig = jax.nn.sigmoid(gpre)
         silu_val = gpre * sig
         hidden = (silu_val * upre).astype(BF16).astype(F32)
@@ -212,9 +262,9 @@
         dhid = weight * qvals
         d_gate = (dhid * upre * sig * (1.0 + gpre * (1.0 - sig))).astype(BF16)
         d_up = (dhid * silu_val).astype(BF16)
-        dg_ref[n] = d_gate
-        du_ref[n] = d_up
-        sc_ref[n] = (weight * hidden).astype(BF16)
+        dg_ref[k] = d_gate
+        du_ref[k] = d_up
+        sc_ref[k] = (weight * hidden).astype(BF16)
         gate_lanes = jnp.where(lane == k, gate_part, 0.0).reshape(n_m, capacity, LANES)
         for at in range(n_m):
             gacc[at % 2, at // 2, :capacity, :] += gate_lanes[at]
@@ -227,25 +277,24 @@
                 back[k, at % 2, at // 2, tp_at] = grad[at]
         remote(back.at[k, 1 - core], core_in.at[k], R1, k, core_to).start()
 
-    group = 2 - experts % 2
-
-    def weight_grads(n, part):
-        tp_at, down = part // 2, part % 2
-        cols = slice(tp_at * share, (tp_at + 1) * share)
-
-        def rows(base):
-            parts = [full[source(n + g), :, tp_at, :, base : base + share] for g in range(group)]
-            return jnp.concatenate([at.reshape(held, share) for at in parts], axis=0)
+    total = experts * held
+    tile = min(share, 512)
+    per = share // tile
+
+    def weight_grads(at, down):
+        cols = slice(at * tile, (at + 1) * tile)
+        base = (at % per) * tile + (share if down else 0)
+        rows = full[:, :, at // per, :, base : base + tile].reshape(total, tile)
 
         def units(ref):
-            return ref[pl.ds(n, group)].reshape(group * held, -1)
+            return ref[...].reshape(total, -1)
 
         if down:
-            gd_ref[0, :, cols] += jnp.dot(units(sc_ref).T, rows(share), preferred_element_type=F32)
+            gd_ref[0, :, cols] = jnp.dot(units(sc_ref).T, rows, preferred_element_type=F32)
         else:
-            flipped = rows(0).T
-            gg_ref[0, cols, :] += jnp.dot(flipped, units(dg_ref), preferred_element_type=F32)
-            gu_ref[0, cols, :] += jnp.dot(flipped, units(du_ref), preferred_element_type=F32)
+            flipped = rows.T
+            gg_ref[0, cols, :] = jnp.dot(flipped, units(dg_ref), preferred_element_type=F32)
+            gu_ref[0, cols, :] = jnp.dot(flipped, units(du_ref), preferred_element_type=F32)
 
     def add(*terms):
         total = terms[0].astype(F32)
@@ -314,49 +363,88 @@
         )
 
     def send_z(i, carry):
-        there = source(i)
-        z_copy(there, e).start()
+        there = source(jnp.where(i == 1, 1, experts + 1 - i))
+        for h in range(2):
+            z_copy(there, e, h).start()
         return carry
 
-    def z_copy(there, at):
+    def z_copy(there, at, h):
         return pltpu.make_async_remote_copy(
-            src_ref=send_ref.at[there],
-            dst_ref=full.at[at, m, t],
-            send_sem=send_sem.at[Z, there],
-            recv_sem=recv_sem.at[Z, at],
+            src_ref=send_ref.at[there, :, parts[h]],
+            dst_ref=full.at[at, m, t, :, parts[h]],
+            send_sem=send_sem.at[Z + h, there],
+            recv_sem=recv_sem.at[Z + h, at],
             device_id=(there, m, t),
             device_id_type=MESH,
         )
 
+    own_here()
     lax.fori_loop(1, experts, send_z, 0)
 
+    def send_weight(d, carry):
+        weight_copy(d).start()
+        return carry
+
+    lax.fori_loop(1, n_ep, send_weight, 0)
+
+    own(source(1), 0)
+    own(source(1), 1)
+    neighbours_here()
+    neighbours(source(1), 0)
+    for load in loads:
+        load.wait()
+
     def step(i, carry):
-        pl.when((i >= 1) & (i < experts + 1))(lambda: neighbours(source(i - 1)))
-        pl.when(i >= 2)(lambda: corners(source(i - 2)))
-        pl.when(i < experts)(lambda: own(source(i), i > 0))
-        pl.when(i >= 3)(lambda: reduce_first(source(i - 3)))
-        pl.when(i >= 4)(lambda: reduce_second(source(i - 4)))
-        pl.when(i >= 5)(lambda: reduce_third(source(i - 5)))
+        at = source(i)
+        own(at, 0)
+        neighbours(source(i - 1), 1)
+        own(at, 1)
+        pl.when(i >= 4)(lambda: reduce_first(source(i - 3)))
+        pl.when(i >= 5)(lambda: reduce_second(source(i - 4)))
+        pl.when(i >= 6)(lambda: reduce_third(source(i - 5)))
 
         @pl.when(i == 2)
         def _():
-            keep.wait()
-            for load in loads:
-                load.wait()
-
-        @pl.when(i >= 2)
+            corners_here()
+            partner_here()
+
+        @pl.when(i > 2)
         def _():
+            corners(source(i - 2))
             partner(source(i - 2))
-            compute(i - 2)
-
-        @pl.when((i >= 1 + group) & (lax.rem(i - 1, group) == 0) & (i < experts + 1))
+
+        compute(source(i - 2))
+        neighbours(at, 0)
+        return carry
+
+    lax.fori_loop(2, experts, step, 0)
+
+    def reduce(stage, n):
+        if n > 0:
+            stage(source(n))
+
+    def close(i, carry):
+        at = source(i)
+
+        @pl.when(i == experts - 2)
         def _():
-            for part in range(2 * n_tp):
-                weight_grads(i - 1 - group, part)
-
+            neighbours(source(experts - 1), 1)
+            reduce(reduce_first, experts - 3)
+            reduce(reduce_second, experts - 4)
+            reduce(reduce_third, experts - 5)
+
+        @pl.when(i == experts - 1)
+        def _():
+            reduce(reduce_second, experts - 3)
+            reduce(reduce_third, experts - 4)
+
+        corners(at)
+        partner(at)
+        pl.when(i == experts - 1)(lambda: reduce_first(source(experts - 2)))
+        compute(at)
         return carry
 
-    lax.fori_loop(0, experts + 2, step, 0)
+    lax.fori_loop(experts - 2, experts, close, 0)
 
     def gate_copy(src, dst, n, device):
         return pltpu.make_async_remote_copy(
@@ -370,29 +458,35 @@
 
     erows = gcore.shape[2]
     last, second, third = [source(experts - n) for n in (1, 2, 3)]
+    rest = [functools.partial(weight_grads, at, down) for at in range(width // tile) for down in (0, 1)]
+    early, late = rest[: len(rest) // 3], rest[len(rest) // 3 :]
+    middle, late = late[: len(rest) // 4], late[len(rest) // 4 :]
     for at in range(n_m):
         gcore[at % 2, at // 2] = gacc[at % 2, at // 2].T[:erows]
     to_core = gate_copy(gcore.at[1 - core], gcore_in, 0, core_to)
     to_core.start()
+    reduce_second(second)
+    reduce_third(third)
     reduce_first(last)
-    rest = [functools.partial(weight_grads, experts - group, part) for part in range(2 * n_tp)]
-    rest.pop()()
+    reduce_first(e)
     to_core.wait_recv()
     gcore[core] = gcore[core] + gcore_in[...]
     to_x = gate_copy(gcore.at[core, x_other], gx_in, 1, x_to)
     to_x.start()
-    reduce_second(second)
-    reduce_third(third)
-    rest.pop()()
+    reduce_third(second)
+    for part in early:
+        part()
+    reduce_second(last)
     to_x.wait_recv()
     gt[t] = gcore[core, x_half] + gx_in[...]
     to_t = [gate_copy(gt.at[t], gt.at[t], 1 + j, (e, m, ahead(j))) for j in range(1, n_tp)]
     for copy in to_t:
         copy.start()
-    reduce_second(last)
-    reduce_third(second)
-    for part in rest:
+    reduce_second(e)
+    for part in middle:
         part()
+    reduce_third(last)
+    reduce_third(e)
     for j in range(1, n_tp):
         gate_copy(gt.at[behind(j)], gt.at[behind(j)], 1 + j, (e, m, ahead(j))).wait_recv()
     whole = gt[0]
@@ -404,6 +498,8 @@
     ]
     for copy in to_z:
         copy.start()
+    for part in late:
+        part()
     for k in range(1, experts):
         src = gz.at[lax.rem(e + experts - k, experts)]
         gate_copy(src, src, n_tp + k, core_to).wait_recv()
@@ -443,7 +539,6 @@
 
     lax.fori_loop(1, n_ep, each, 0)
 
-    reduce_third(last)
     weight_rows = [rw_ref[:, mine_cols].astype(F32)] + ([jnp.zeros((pad, share), F32)] if pad else [])
     router_part = lax.dot_general(
         dlog, jnp.concatenate(weight_rows, axis=0), (((0,), (0,)), ((), ())), precision=HIGHEST, preferred_element_type=F32
@@ -463,6 +558,7 @@
 
     def done(d, carry):
         term_copy(d).wait_send()
+        weight_copy(d).wait_send()
         return carry
 
     lax.fori_loop(1, n_ep, done, 0)
@@ -474,22 +570,33 @@
 
         @pl.when(k != e)
         def _():
-            sent(mine, Z, k)
             sent(mine_back(k), RET, k)
-
-        sent(mine, X, k)
-        sent(mine, CORE_OWN, k)
-        sent(piece(k, x_peer, t), CORE_X, k)
+            for h, cols in enumerate(parts):
+                mine_part = piece(k, m, t, cols)
+                sent(mine_part, Z + h, k)
+                sent(mine_part, X + h, k)
+                sent(mine_part, CORE_OWN + h, k)
+                sent(mine_part, CORE_X + h, k)
+                for j in range(1, n_tp):
+                    sent(mine_part, y_kind(j) + h, k)
+                    sent(mine_part, core_y(j) + h, k)
+            for j in range(1, n_tp):
+                for kind in (a_kind, b_kind, core_a, core_b):
+                    sent(piece(k, m, t, first_cols), kind(j), k)
+
+        @pl.when(k == e)
+        def _():
+            sent(mine, X, e)
+            sent(full.at[e, m], CORE_OWN, e)
+            sent(mine, CORE_X, e)
+            for j in range(1, n_tp):
+                for kind in (a_kind, b_kind, core_a, core_b):
+                    sent(piece(e, m, t, first_cols), kind(j), e)
+
         sent(core_in.at[k], R1, k)
         sent(across_a(k), R2A, k)
         sent(onward_b(k), R3B, k)
         for j in range(1, n_tp):
-            sent(mine, y_kind(j), k)
-            sent(piece(k, x_peer, t, last_cols), b_kind(j), k)
-            sent(piece(k, m, behind(j), first_cols), a_kind(j), k)
-            sent(piece(k, m, behind(j)), core_y(j), k)
-            sent(piece(k, x_peer, behind(j), first_cols), core_a(j), k)
-            sent(piece(k, x_peer, behind(j), last_cols), core_b(j), k)
             sent(across_b(k, j), r2b(j), k)
             sent(onward_a(k, j), r3a(j), k)
         return carry
@@ -518,11 +625,11 @@
     capacity = -(-capacity // 16) * 16
     ff = gate_proj.shape[2]
 
-    wide = 2 * share + LANES
+    wide = 2 * share
     held = n_m * capacity
     hid_shape = jax.ShapeDtypeStruct((experts, held, ff), BF16)
     flops = 2 * experts * held * width * ff
-    kinds = 8 + 8 * (n_tp - 1)
+    kinds = 12 + 10 * (n_tp - 1)
     n_ep = experts * n_m
     half = share // 2
     erows = -(-experts // 8) * 8
@@ -544,6 +651,8 @@
         ],
         scratch_shapes=[
             pltpu.VMEM((experts, capacity, wide), BF16),
+            pltpu.VMEM((experts, 8, LANES), F32),
+            pltpu.VMEM((n_ep, 8, LANES), F32),
             pltpu.VMEM(full_shape, BF16),
             pltpu.VMEM(gate_proj.shape, BF16),
             pltpu.VMEM(up_proj.shape, BF16),
@@ -574,6 +683,8 @@
             pltpu.SemaphoreType.DMA((n_tp + experts,)),
             pltpu.SemaphoreType.DMA((n_ep,)),
             pltpu.SemaphoreType.DMA((n_ep,)),
+            pltpu.SemaphoreType.DMA((n_ep,)),
+            pltpu.SemaphoreType.DMA((n_ep,)),
         ],
         compiler_params=pltpu.CompilerParams(
             collective_id=0, has_side_effects=True, vmem_limit_bytes=46 << 20

time: 111 us -> 105 us (0.946)
  Pallas kernels: 110 us -> 104 us
    pallas_call x1, Pallas kernels: 105 us -> 99.4 us  [shards(): pl.pallas_call(functools.partial(rows_kernel, share), in_specs=[vmem] * 4...]
where the time goes in v3:
time: 105 us
  Pallas kernels  104 us (99%)
    pallas_call x1, Pallas kernels, shards(): pl.pallas_call(functools.partial(rows_kernel, share), in_specs=[vmem] * 4...  99.4 us
    pallas_call x1, Pallas kernels, shards(): pl.pallas_call(hand_over, in_specs=[vmem] * 6, out_specs=[anywhere] * 6,...  4.72 us

profile of v3, /device:TPU:0, one launch (start us, length us, event | category | flops | bytes accessed | tf_op | source)
XLA Modules:
  0.0 105.0 jit_solution(9246265876830968646)
XLA Ops:
  0.6 99.4 %rows.1 = (f32[1,2048,512]{2,1,0:T(8,128)S(1)}, f32[1,2048,512]{2,1,0:T(8,128)S(1)}, f32[1,512,2048]{2,1,0:T(8,128)S(1)}, bf16[128,1024]{1,0:T(8,128)(2,1)S(1)},...) custom-call(bf16[128,2048]{1,0:T(8,128)(2,1)} %tok_ref.1, bf16[128,2048]{1,0:T(8,128)(2,1)} %cot_ref.1, s32[2,128]{1,0:T(2,128)} %bitcast.6, ...), custom_call_target="tpu_custom_call" | custom-call | flops 13421772800 | bytes 31457280 | tf_op jit(solution)/shard_map/rows/pallas_call | solution.py:640
  100.1 4.7 %hand_over.1 = (f32[1,2048,512]{2,1,0:T(8,128)}, f32[1,2048,512]{2,1,0:T(8,128)}, f32[1,512,2048]{2,1,0:T(8,128)}, bf16[128,1024]{1,0:T(8,128)(2,1)}, f32[2,128]{1,0:T(2,128)}, /*index=5*/f32[4,128]{1,0:T(4,128)}) custom-call(f32[1,2048,512]{2,1,0:T(8,128)S(1)} %get-tuple-element.18.refs_0_, f32[1,2048,512]{2,1,0:T(8,128)S(1)} %get-tuple-element.19.refs_1_, ...), custom_call_target="tpu_custom_call" | custom-call | tf_op jit(solution)/shard_map/hand_over/pallas_call | solution.py:705

commit v4 on v3

--- a/solution.py
+++ b/solution.py
@@ -364,6 +364,7 @@
 
     def send_z(i, carry):
         there = source(jnp.where(i == 1, 1, experts + 1 - i))
+
         for h in range(2):
             z_copy(there, e, h).start()
         return carry
@@ -378,8 +379,12 @@
             device_id_type=MESH,
         )
 
+    def send_far():
+        lax.fori_loop(2, experts, send_z, 0)
+
     own_here()
-    lax.fori_loop(1, experts, send_z, 0)
+    send_z(1, 0)
+    pl.when(near > 0)(send_far)
 
     def send_weight(d, carry):
         weight_copy(d).start()
@@ -391,13 +396,15 @@
     own(source(1), 1)
     neighbours_here()
     neighbours(source(1), 0)
+    pl.when(near == 0)(send_far)
+    neighbours(source(1), 1)
     for load in loads:
         load.wait()
 
     def step(i, carry):
         at = source(i)
         own(at, 0)
-        neighbours(source(i - 1), 1)
+        pl.when(i > 2)(lambda: neighbours(source(i - 1), 1))
         own(at, 1)
         pl.when(i >= 4)(lambda: reduce_first(source(i - 3)))
         pl.when(i >= 5)(lambda: reduce_second(source(i - 4)))
@@ -468,12 +475,12 @@
     reduce_second(second)
     reduce_third(third)
     reduce_first(last)
-    reduce_first(e)
     to_core.wait_recv()
     gcore[core] = gcore[core] + gcore_in[...]
     to_x = gate_copy(gcore.at[core, x_other], gx_in, 1, x_to)
     to_x.start()
     reduce_third(second)
+    reduce_first(e)
     for part in early:
         part()
     reduce_second(last)
@@ -498,8 +505,6 @@
     ]
     for copy in to_z:
         copy.start()
-    for part in late:
-        part()
     for k in range(1, experts):
         src = gz.at[lax.rem(e + experts - k, experts)]
         gate_copy(src, src, n_tp + k, core_to).wait_recv()
@@ -538,6 +543,8 @@
         return carry
 
     lax.fori_loop(1, n_ep, each, 0)
+    for part in late:
+        part()
 
     weight_rows = [rw_ref[:, mine_cols].astype(F32)] + ([jnp.zeros((pad, share), F32)] if pad else [])
     router_part = lax.dot_general(

time: 105 us -> 99.6 us (0.949)
  Pallas kernels: 104 us -> 98.7 us
    pallas_call x1, Pallas kernels: 99.4 us -> 93.9 us  [shards(): pl.pallas_call(functools.partial(rows_kernel, share), in_specs=[vmem] * 4...]
where the time goes in v4:
time: 99.6 us; the launch traced here: 99.5 us
  Pallas kernels  98.7 us (99%)
    pallas_call x1, Pallas kernels, shards(): pl.pallas_call(functools.partial(rows_kernel, share), in_specs=[vmem] * 4...  93.9 us
    pallas_call x1, Pallas kernels, shards(): pl.pallas_call(hand_over, in_specs=[vmem] * 6, out_specs=[anywhere] * 6,...  4.72 us

profile of v4, /device:TPU:0, one launch (start us, length us, event | category | flops | bytes accessed | tf_op | source)
XLA Modules:
  0.0 99.5 jit_solution(11465309616481481387)
XLA Ops:
  0.6 93.9 %rows.1 = (f32[1,2048,512]{2,1,0:T(8,128)S(1)}, f32[1,2048,512]{2,1,0:T(8,128)S(1)}, f32[1,512,2048]{2,1,0:T(8,128)S(1)}, bf16[128,1024]{1,0:T(8,128)(2,1)S(1)},...) custom-call(bf16[128,2048]{1,0:T(8,128)(2,1)} %tok_ref.1, bf16[128,2048]{1,0:T(8,128)(2,1)} %cot_ref.1, s32[2,128]{1,0:T(2,128)} %bitcast.6, ...), custom_call_target="tpu_custom_call" | custom-call | flops 13421772800 | bytes 31457280 | tf_op jit(solution)/shard_map/rows/pallas_call | solution.py:647
  94.6 4.7 %hand_over.1 = (f32[1,2048,512]{2,1,0:T(8,128)}, f32[1,2048,512]{2,1,0:T(8,128)}, f32[1,512,2048]{2,1,0:T(8,128)}, bf16[128,1024]{1,0:T(8,128)(2,1)}, f32[2,128]{1,0:T(2,128)}, /*index=5*/f32[4,128]{1,0:T(4,128)}) custom-call(f32[1,2048,512]{2,1,0:T(8,128)S(1)} %get-tuple-element.18.refs_0_, f32[1,2048,512]{2,1,0:T(8,128)S(1)} %get-tuple-element.19.refs_1_, ...), custom_call_target="tpu_custom_call" | custom-call | tf_op jit(solution)/shard_map/hand_over/pallas_call | solution.py:712
